TPU v7x, 512 devices: a whole 4x8x8 slice. The times are simulated.
512 devices in a mesh: dp: 4 (over x), kv: 64 (over z, y), tp: 2 (over core).
Axes of the slice: x: 4, y: 8, z: 8, core: 2. Of those that a mesh axis runs over, the one named last changes fastest.
Arguments:
- tokens: bfloat16 [64, 16, 2048], P('dp'), may hold values from -6 to 6
- norm_gain: float32 [2048], replicated, may hold values from 0.1 to 1.9
- query_weight: bfloat16 [2048, 1024], P(None, 'tp'), may hold values from -0.125 to 0.125
- key_weight: bfloat16 [2048, 256], P(None, 'tp'), may hold values from -0.125 to 0.125
- value_weight: bfloat16 [2048, 256], P(None, 'tp'), may hold values from -0.125 to 0.125
- forget_weight: bfloat16 [2048, 8], replicated, may hold values from -0.125 to 0.125
- forget_bias: float32 [8], replicated, may hold values from 0 to 4
- query_gain: float32 [128], replicated, may hold values from 0.1 to 1.9
- key_gain: float32 [128], replicated, may hold values from 0.1 to 1.9
- output_weight: bfloat16 [1024, 2048], P('tp', 'kv'), may hold values from -0.1875 to 0.1875
- cache_keys: bfloat16 [64, 16384, 2, 128], P('dp', 'kv', 'tp'), may hold values from -512 to 512
- cache_values: bfloat16 [64, 16384, 2, 128], P('dp', 'kv', 'tp'), may hold values from -6 to 6
- cache_logcum: float32 [64, 16384, 8], P('dp', 'kv', 'tp'), may hold values from -3277 to 0, as said below
- pending_keys: bfloat16 [64, 4, 2, 128], P('dp', None, 'tp'), may hold values from -6 to 6
- pending_values: bfloat16 [64, 4, 2, 128], P('dp', None, 'tp'), may hold values from -6 to 6
- pending_logcum: float32 [64, 4, 8], P('dp', None, 'tp'), may hold values from -3277 to 0, as said below
- lengths: int32 [64], P('dp'), may hold values from 8192 to 16380, as said below
- accepted: int32 [64], P('dp'), may hold values from 1 to 4
- parents: int32 [64, 16], P('dp'), may hold values from -1 to 14, as said below
Outputs:
- result: bfloat16 [64, 16, 2048], P('dp', None, ('kv', 'tp'))
Inputs may be any that keep to these rules, and one draw needn't show every extreme that they name: Positions below lengths hold a sequence's past; the last step's accepted proposals go to positions lengths to lengths + accepted - 1. `parents`: the parent of proposal i is -1 (the last accepted token) or a proposal before i. `cache_logcum`: non-increasing along positions for every sequence and head. `pending_logcum`: the cumulative log gates at positions lengths to lengths + 3, continuing cache_logcum.
All inputs are finite; a program needn't handle non-finite values.
Results may differ from a plain program's by a relative error of at most 0.014.
Values may be sent and summed in bfloat16 or wider, within the bound.
A program may use at most 128 MiB of HBM per device.

v0:
```python
import jax
import jax.numpy as jnp
from jax import lax
from jax.sharding import PartitionSpec as P

EPSILON = 1e-06
NEG_LARGE = -1e30
HIGHEST = lax.Precision.HIGHEST


def copy_for_each(shard, axis):
    size = lax.axis_size(axis)
    return lax.all_to_all(
        jnp.broadcast_to(shard[None], (size, *shard.shape)), axis, 0, 0, tiled=True
    )


def over_copies(shard, axis):
    return copy_for_each(shard, axis).max(axis=0)


def in_blocks(shard, dim, size):
    before, after = (shard.shape[:dim], shard.shape[dim + 1 :])
    return jnp.moveaxis(shard.reshape(*before, size, -1, *after), dim, 0)


def summed_on_arrival(shard, axis, dim):
    size = lax.axis_size(axis)
    blocks = lax.all_to_all(in_blocks(shard, dim, size), axis, 0, 0, tiled=True)
    return jnp.sum(blocks.astype(jnp.float32), axis=0)


def side_by_side(arrays, axis, dim, along):
    columns = [a.reshape(*a.shape[:along], -1) for a in arrays]
    both = jnp.concatenate(columns, axis=along)
    whole, at, done = (summed_on_arrival(both, axis, dim), 0, [])
    for a, column in zip(arrays, columns):
        section = whole[..., at : at + column.shape[along]]
        done.append(section.reshape(*section.shape[:along], *a.shape[along:]))
        at += column.shape[along]
    return tuple(done)


def joined_along(blocks, dim):
    blocks = jnp.moveaxis(blocks, 0, dim)
    dims = blocks.shape
    return blocks.reshape(*dims[:dim], dims[dim] * dims[dim + 1], *dims[dim + 2 :])


def gathered_copies(shard, axis, dim):
    return joined_along(copy_for_each(shard, axis), dim)


def head_norm(vectors, gain_vec):
    return (
        vectors
        * lax.rsqrt(jnp.mean(vectors * vectors, axis=-1, keepdims=True) + EPSILON)
        * gain_vec
    )


def ancestors(parents):
    node_count = parents.shape[-1]
    indices = jnp.arange(node_count, dtype=jnp.int32)
    reachable = (parents[..., None] == indices).astype(jnp.float32) + jnp.eye(
        node_count, dtype=jnp.float32
    )
    for doubling in range((node_count - 1).bit_length()):
        reachable = jnp.minimum(
            jnp.einsum("sij,sjk->sik", reachable, reachable, precision=HIGHEST), 1.0
        )
    return reachable


def to_rows(values):
    moved = jnp.swapaxes(values, 1, 2)
    return moved.reshape((moved.shape[0] * moved.shape[1],) + moved.shape[2:])


def finish_rows(cache_max, cache_sum, cache_acc, tree_max, tree_sum, tree_acc):
    overall = jnp.maximum(cache_max, tree_max)
    factor_cache = jnp.exp(cache_max - overall)
    factor_tree = jnp.exp(tree_max - overall)
    denominator = cache_sum * factor_cache + tree_sum * factor_tree
    numerator = cache_acc * factor_cache[..., None] + tree_acc * factor_tree[..., None]
    attended = (numerator / denominator[..., None]).astype(jnp.bfloat16)
    return attended.reshape(attended.shape[0], attended.shape[1] * attended.shape[2])


def shards(
    tokens,
    norm_gain,
    query_weight,
    key_weight,
    value_weight,
    forget_weight,
    forget_bias,
    query_gain,
    key_gain,
    output_weight,
    cache_keys,
    cache_values,
    cache_logcum,
    pending_keys,
    pending_values,
    pending_logcum,
    lengths,
    accepted,
    parents,
):
    seq_count, node_count, model_width = tokens.shape
    token_rows = seq_count * node_count
    head_size = query_gain.shape[0]
    query_cols = query_weight.shape[1]
    key_cols = key_weight.shape[1]
    local_heads = query_cols // head_size
    key_heads = key_cols // head_size
    sharing = local_heads // key_heads
    block_len = cache_keys.shape[1]
    most_taken = pending_keys.shape[1]
    scaling = head_size ** (-0.5)
    widened = tokens.reshape(token_rows, model_width).astype(jnp.float32)
    normed = (
        widened
        * lax.rsqrt(jnp.mean(widened * widened, axis=-1, keepdims=True) + EPSILON)
        * norm_gain
    ).astype(jnp.bfloat16)
    joined_weight = jnp.concatenate([query_weight, key_weight, value_weight], axis=1)
    summed = jnp.dot(normed, joined_weight, preferred_element_type=jnp.float32)
    query_part = head_norm(
        summed[:, :query_cols].reshape(token_rows, local_heads, head_size), query_gain
    )
    key_part = head_norm(
        summed[:, query_cols : query_cols + key_cols].reshape(token_rows, key_heads, head_size),
        key_gain,
    )
    queries = query_part.astype(jnp.bfloat16).reshape(
        seq_count, node_count, key_heads, sharing, head_size
    )
    keys_new = key_part.astype(jnp.bfloat16).reshape(seq_count, node_count, key_heads, head_size)
    values_new = (
        summed[:, query_cols + key_cols :]
        .astype(jnp.bfloat16)
        .reshape(seq_count, node_count, key_heads, head_size)
    )
    head_start = lax.axis_index("tp") * local_heads
    forget_cols = lax.dynamic_slice_in_dim(forget_weight, head_start, local_heads, 1)
    gate_bias = lax.dynamic_slice_in_dim(forget_bias, head_start, local_heads, 0)
    log_gates = jax.nn.log_sigmoid(
        jnp.dot(normed, forget_cols, preferred_element_type=jnp.float32) + gate_bias
    ).reshape(seq_count, node_count, local_heads)
    ancestry = ancestors(parents)
    choose = (jnp.arange(most_taken, dtype=jnp.int32)[None, :] == (accepted - 1)[:, None]).astype(
        jnp.float32
    )
    base_gate = jnp.einsum("sa,sah->sh", choose, pending_logcum, precision=HIGHEST)
    cumulative = base_gate[:, None, :] + jnp.einsum(
        "sij,sjh->sih", ancestry, log_gates, precision=HIGHEST
    )
    gate_rows = jnp.swapaxes(cumulative, 1, 2)
    token_place = lax.axis_index("kv") * block_len + jnp.arange(block_len, dtype=jnp.int32)
    offset = token_place[None, :] - lengths[:, None]
    inserted = (offset >= 0) & (offset < accepted[:, None])
    one_hot = (offset[..., None] == jnp.arange(most_taken, dtype=jnp.int32)) & inserted[..., None]
    hot_low = one_hot.astype(jnp.bfloat16)
    merged_keys = jnp.where(
        inserted[..., None, None],
        jnp.einsum(
            "sla,sakd->slkd", hot_low, pending_keys, preferred_element_type=jnp.float32
        ).astype(jnp.bfloat16),
        cache_keys,
    )
    merged_values = jnp.where(
        inserted[..., None, None],
        jnp.einsum(
            "sla,sakd->slkd", hot_low, pending_values, preferred_element_type=jnp.float32
        ).astype(jnp.bfloat16),
        cache_values,
    )
    log_cache = jnp.where(
        inserted[..., None],
        jnp.einsum("sla,sah->slh", one_hot.astype(jnp.float32), pending_logcum, precision=HIGHEST),
        cache_logcum,
    )
    usable = token_place[None, :] < (lengths + accepted)[:, None]
    raw_scores = jnp.einsum(
        "spkgd,slkd->skgpl", queries, merged_keys, preferred_element_type=jnp.float32
    )
    scores = (
        raw_scores.reshape(seq_count, local_heads, node_count, block_len) * scaling
        + gate_rows[..., None]
        - jnp.swapaxes(log_cache, 1, 2)[:, :, None, :]
    )
    visible = usable[:, None, None, :]
    block_max = jnp.max(jnp.where(visible, scores, NEG_LARGE), axis=-1)
    weights = jnp.where(visible, jnp.exp(scores - block_max[..., None]), 0.0)
    block_sum = jnp.sum(weights, axis=-1)
    block_acc = jnp.einsum(
        "skgpl,slkd->skgpd",
        weights.astype(jnp.bfloat16).reshape(seq_count, key_heads, sharing, node_count, block_len),
        merged_values,
        preferred_element_type=jnp.float32,
    )
    block_acc = block_acc.reshape(seq_count, local_heads, node_count, head_size)
    tree_raw = jnp.einsum(
        "spkgd,sjkd->skgpj", queries, keys_new, preferred_element_type=jnp.float32
    )
    tree_scores = (
        tree_raw.reshape(seq_count, local_heads, node_count, node_count) * scaling
        + gate_rows[..., :, None]
        - gate_rows[..., None, :]
    )
    tree_mask = ancestry[:, None] > 0.5
    tree_max = jnp.max(jnp.where(tree_mask, tree_scores, NEG_LARGE), axis=-1)
    tree_weights = jnp.where(tree_mask, jnp.exp(tree_scores - tree_max[..., None]), 0.0)
    tree_sum = jnp.sum(tree_weights, axis=-1)
    tree_acc = jnp.einsum(
        "skgpj,sjkd->skgpd",
        tree_weights.astype(jnp.bfloat16).reshape(
            seq_count, key_heads, sharing, node_count, node_count
        ),
        values_new,
        preferred_element_type=jnp.float32,
    )
    tree_acc = tree_acc.reshape(seq_count, local_heads, node_count, head_size)
    tree_max_rows = to_rows(tree_max)
    tree_sum_rows = to_rows(tree_sum)
    tree_acc_rows = to_rows(tree_acc)
    cache_max = over_copies(block_max, "kv")
    rescale = jnp.exp(block_max - cache_max)
    own_sum, own_acc = side_by_side(
        (
            to_rows(block_sum * rescale).astype(jnp.bfloat16),
            to_rows(block_acc * rescale[..., None]).astype(jnp.bfloat16),
        ),
        "kv",
        0,
        2,
    )
    share = own_sum.shape[0]
    row_start = lax.axis_index("kv") * share

    def own(values):
        return lax.dynamic_slice_in_dim(values, row_start, share, 0)

    own_attended = finish_rows(
        own(to_rows(cache_max)),
        own_sum,
        own_acc,
        own(tree_max_rows),
        own(tree_sum_rows),
        own(tree_acc_rows),
    )
    attended = gathered_copies(own_attended, "kv", 0)
    head_part = jnp.dot(attended, output_weight, preferred_element_type=jnp.float32)
    head_part = head_part.reshape(seq_count, node_count, output_weight.shape[1])
    return summed_on_arrival(head_part.astype(jnp.bfloat16), "tp", 2).astype(jnp.bfloat16)


def solution(mesh):
    placed = (
        P("dp", None, None),
        P(),
        P(None, "tp"),
        P(None, "tp"),
        P(None, "tp"),
        P(),
        P(),
        P(),
        P(),
        P("tp", "kv"),
        P("dp", "kv", "tp", None),
        P("dp", "kv", "tp", None),
        P("dp", "kv", "tp"),
        P("dp", None, "tp", None),
        P("dp", None, "tp", None),
        P("dp", None, "tp"),
        P("dp"),
        P("dp"),
        P("dp", None),
    )
    return jax.shard_map(
        shards, mesh=mesh, in_specs=placed, out_specs=P("dp", None, ("kv", "tp")), check_vma=False
    )
```

profile of v0, /device:TPU:1, one launch (start us, length us, event | category | flops | bytes accessed | tf_op | source)
XLA Modules:
  0.0 108.1 jit_solution(8813294599660406562)
XLA Ops:
  0.1 0.8 fusion.92
  1.6 0.7 broadcast_compare_fusion.1
  2.4 1.5 %multiply_reduce_fusion = f32[16,16]{1,0:T(8,128)S(1)} fusion(bf16[16,16,2048]{2,1,0:T(8,128)(2,1)} %param.19), kind=kLoop, calls=%fused_computation.9 | loop fusion | flops 1572608 | bytes 1049600 | tf_op jit(solution)/shard_map/reduce_sum | solution.py:125
  4.0 0.8 copy.165
  4.8 1.1 %convolution_minimum_fusion.3 = f32[16,16,16]{2,1,0:T(8,128)S(1)} fusion(f32[16,16]{1,0:T(8,128)S(1)} %fusion.71, s32[16,16]{1,0:T(8,128)} %param.37), kind=kOutput, calls=%fused_computation.23 | convolution fusion | flops 802816 | bytes 18432 | tf_op jit(solution)/shard_map/sij,sjk->sik/dot_general | solution.py:70
  7.6 2.7 %fusion = f32[256,768]{1,0:T(8,128)S(1)} fusion(bf16[256,2048]{1,0:T(8,128)(2,1)S(1)} %fusion.7, bf16[2048,128]{1,0:T(8,128)(2,1)S(1)} %copy-done.19, bf16[2048,128]{1,0:T(8,128)(2,1)} %param.22, bf16[2048,512]{1,0:T(8,128)(2,1)} %param.21), kind=kOutput, calls=%fused_computation | convolution fusion | flops 814743552 | bytes 4980736 | tf_op jit(solution)/shard_map/dot_general | solution.py:129
  10.6 0.7 copy-done.2
  13.0 3.0 %select_reduce_fusion.1 = (f32[16,4,16]{2,1,0:T(4,128)S(1)}, f32[16,256,16,4]{1,2,3,0:T(8,128)S(1)}) fusion(f32[16,4,256]{2,1,0:T(4,128)S(1)} %fusion.12, f32[16,4,16]{2,1,0:T(4,128)S(1)} %convolution_add_fusion, pred[16,256]{1,0:T(8,128)(4,1)S(1)} %get-tuple-element.12, f32[16,16,4,128]{3,2,1,0:T(4,128)S(1)} %reshape.345, f32[128]{0:T(128)S(1)} %copy-done.23, ...), kind=kOutput, calls=%fused_computation.46 | convolution fusion | flops 74087424 | bytes 2740736 | tf_op jit(solution)/shard_map/spkgd,slkd->skgpl/dot_general | solution.py:186
  16.6 2.3 %reshape.367 = f32[64,1,1024]{2,1,0:T(1,128)} reshape(f32[64,16,4,16]{3,2,1,0:T(4,128)S(1)} %broadcast_in_dim.114) | data formatting | bytes 524288
  18.9 17.3 %all-to-all-start = ((f32[64,1,1024]{2,1,0:T(1,128)}), f32[64,1,1024]{2,1,0:T(1,128)S(1)}, u32[]{:S(2)}, u32[]{:S(2)}) async-start(f32[64,1,1024]{2,1,0:T(1,128)} %reshape.367), calls=%async_computation | async-start | bytes 524288 | tf_op jit(solution)/shard_map/all_to_all | solution.py:13
  36.4 1.2 %select_reduce_fusion = f32[16,4,16]{2,1,0:T(4,128)} fusion(f32[16,256,16,4]{1,2,3,0:T(8,128)S(1)} %get-tuple-element.17, f32[16,4,16]{2,1,0:T(4,128)S(1)} %get-tuple-element.16, f32[16,4,256]{2,1,0:T(4,128)S(1)} %fusion.12, f32[16,4,16]{2,1,0:T(4,128)S(1)} %convolution_add_fusion, pred[16,256]{1,0:T(8,128)(4,1)S(1)} %get-tuple-element.12), kind=kLoop, calls=%fused_computation.45 | loop fusion | flops 1309696 | bytes 1130496 | tf_op jit(solution)/shard_map/reduce_sum | solution.py:197
  37.5 1.0 multiply_reduce_fusion.1
  38.6 1.6 %multiply_convert_fusion = bf16[256,128]{1,0:T(8,128)(2,1)} fusion(f32[256,768]{1,0:T(8,128)} %copy-done.2, f32[128]{0:T(128)S(1)} %copy-done.18, f32[256]{0:T(256)S(1)} %add_rsqrt_fusion.2), kind=kLoop, calls=%fused_computation.78 | loop fusion | flops 98304 | bytes 198144 | tf_op jit(solution)/shard_map/convert_element_type | solution.py:140
  40.2 8.6 %all-to-all-done = f32[64,1,1024]{2,1,0:T(1,128)S(1)} async-done(((f32[64,1,1024]{2,1,0:T(1,128)}), f32[64,1,1024]{2,1,0:T(1,128)S(1)}, u32[]{:S(2)}, u32[]{:S(2)}) %all-to-all-start) | async-done | bytes 262176 | tf_op jit(solution)/shard_map/all_to_all | solution.py:13
  49.4 1.3 %reduce.4 = f32[64,1024]{1,0:T(8,128)S(1)} reduce(f32[64,1,1024]{2,1,0:T(1,128)S(1)} %all-to-all-done, f32[]{:T(128)} %broadcast.228), dimensions={1}, to_apply=%all_to_all.12.reduce_sub_computation | reduce | bytes 524292 | tf_op jit(solution)/shard_map/all_to_all | solution.py:13
  50.7 1.5 %reshape.368 = f32[64,16,4,16]{3,2,1,0:T(4,128)S(1)} reshape(f32[64,1024]{1,0:T(8,128)S(1)} %reduce.4) | data formatting | bytes 524288
  53.1 2.9 %fusion.11 = bf16[16,16,4,128]{3,1,2,0:T(8,128)(2,1)S(1)} fusion(bf16[16,256,1,128]{3,1,2,0:T(8,128)(2,1)} %param.30, pred[16,256]{1,0:T(8,128)(4,1)S(1)} %copy-done.15, f32[16,256,16,4]{1,2,3,0:T(8,128)S(1)} %get-tuple-element.17, f32[16,4,16]{2,1,0:T(4,128)S(1)} %get-tuple-element.16, f32[16,4,256]{2,1,0:T(4,128)S(1)} %copy-done.6, ...), kind=kOutput, calls=%fused_computation.19 | convolution fusion | flops 73957376 | bytes 2478080 | tf_op jit(solution)/shard_map/skgpl,slkd->skgpd/dot_general | solution.py:198
  56.9 1.0 copy.171
  57.9 5.7 %all-to-all-start.1 = ((bf16[64,4,4,129]{3,1,2,0:T(4,128)(2,1)}), bf16[64,4,4,129]{3,1,2,0:T(4,128)(2,1)S(1)}, u32[]{:S(2)}, u32[]{:S(2)}) async-start(bf16[64,4,4,129]{3,1,2,0:T(4,128)(2,1)} %copy.171), calls=%async_computation.1 | async-start | bytes 1048576 | tf_op jit(solution)/shard_map/all_to_all | solution.py:29
  63.6 0.8 select_reduce_fusion.3
  64.4 0.9 slice.39
  66.5 12.7 %all-to-all-done.1 = bf16[64,4,4,129]{3,1,2,0:T(4,128)(2,1)S(1)} async-done(((bf16[64,4,4,129]{3,1,2,0:T(4,128)(2,1)}), bf16[64,4,4,129]{3,1,2,0:T(4,128)(2,1)S(1)}, u32[]{:S(2)}, u32[]{:S(2)}) %all-to-all-start.1) | async-done | bytes 264224 | tf_op jit(solution)/shard_map/all_to_all | solution.py:29
  79.9 19.9 %all_to_all.20 = bf16[64,4,512]{2,1,0:T(4,128)(2,1)S(1)} all-to-all(bf16[64,4,512]{2,1,0:T(4,128)(2,1)S(1)} %broadcast_in_dim.123), channel_id=1, replica_groups=mesh['dp'=4,'kv'=64,'tp'=2] {'kv'}, dimensions={0} | all-to-all | bytes 524288 | tf_op jit(solution)/shard_map/all_to_all | solution.py:13
  100.4 6.9 %all_to_all.21 = bf16[2,2,2048]{2,1,0:T(2,128)(2,1)S(1)} all-to-all(bf16[2,2,2048]{2,1,0:T(2,128)(2,1)S(1)} %reshape.369), channel_id=1, replica_groups=mesh['dp'=4,'kv'=64,'tp'=2] {'tp'}, dimensions={0} | all-to-all | bytes 32768 | tf_op jit(solution)/shard_map/all_to_all | solution.py:29
  (103 shorter events, 10.4 us)
Async XLA Ops:
  0.0 99.9 %copy-start = (bf16[512,32]{0,1:T(8,128)(2,1)S(1)}, bf16[512,32]{0,1:T(8,128)(2,1)}, u32[]{:S(2)}) copy-start(bf16[512,32]{0,1:T(8,128)(2,1)} %param.28) | copy-start | bytes 98308
  0.0 6.8 %copy-start.1 = (bf16[16,16,2048]{2,1,0:T(8,128)(2,1)S(1)}, bf16[16,16,2048]{2,1,0:T(8,128)(2,1)}, u32[]{:S(2)}) copy-start(bf16[16,16,2048]{2,1,0:T(8,128)(2,1)} %param.19) | copy-start | bytes 3145732
  0.0 6.7 %copy-start.22 = (f32[8]{0:T(128)S(1)}, f32[8]{0:T(128)}, u32[]{:S(2)}) copy-start(f32[8]{0:T(128)} %param.25) | copy-start | bytes 100
  0.0 6.8 %copy-start.17 = (f32[2048]{0:T(1024)S(1)}, f32[2048]{0:T(1024)}, u32[]{:S(2)}) copy-start(f32[2048]{0:T(1024)} %param.20) | copy-start | bytes 24580
  2.4 10.6 %copy-start.14 = (pred[16,256]{1,0:T(8,128)(4,1)}, pred[16,256]{1,0:T(8,128)(4,1)S(1)}, u32[]{:S(2)}) copy-start(pred[16,256]{1,0:T(8,128)(4,1)S(1)} %get-tuple-element.13) | copy-start | bytes 12292
  2.4 34.0 %copy-start.12 = (pred[16,256]{1,0:T(8,128)(4,1)}, pred[16,256]{1,0:T(8,128)(4,1)S(1)}, u32[]{:S(2)}) copy-start(pred[16,256]{1,0:T(8,128)(4,1)S(1)} %get-tuple-element.12) | copy-start | bytes 12292
  2.4 4.8 %copy-start.16 = (bf16[2048,8]{0,1:T(8,128)(2,1)S(1)}, bf16[2048,8]{0,1:T(8,128)(2,1)}, u32[]{:S(2)}) copy-start(bf16[2048,8]{0,1:T(8,128)(2,1)} %param.24) | copy-start | bytes 98308
  6.2 1.4 %copy-start.19 = (bf16[2048,128]{1,0:T(8,128)(2,1)S(1)}, bf16[2048,128]{1,0:T(8,128)(2,1)}, u32[]{:S(2)}) copy-start(bf16[2048,128]{1,0:T(8,128)(2,1)} %param.23) | copy-start | bytes 1572868
  10.4 0.9 copy-start.2
  10.4 2.0 %copy-start.8 = (f32[16,256,4]{1,2,0:T(4,128)S(1)}, f32[16,256,4]{1,2,0:T(4,128)}, u32[]{:S(2)}) copy-start(f32[16,256,4]{1,2,0:T(4,128)} %param.31) | copy-start | bytes 196612
  11.3 1.7 %copy-start.20 = (bf16[16,4,1,128]{3,1,2,0:T(4,128)(2,1)S(1)}, bf16[16,4,1,128]{3,1,2,0:T(4,128)(2,1)}, u32[]{:S(2)}) copy-start(bf16[16,4,1,128]{3,1,2,0:T(4,128)(2,1)} %param.32) | copy-start | bytes 49156
  11.3 1.7 %copy-start.23 = (f32[128]{0:T(128)S(1)}, f32[128]{0:T(128)}, u32[]{:S(2)}) copy-start(f32[128]{0:T(128)} %param.26) | copy-start | bytes 1540
  12.0 4.1 %copy-start.10 = (f32[16,16,4]{1,2,0:T(4,128)}, f32[16,16,4]{1,2,0:T(4,128)S(1)}, u32[]{:S(2)}) copy-start(f32[16,16,4]{1,2,0:T(4,128)S(1)} %copy.162) | copy-start | bytes 12292
  12.2 3.9 %copy-start.3 = (f32[16,16,4,128]{3,2,1,0:T(4,128)}, f32[16,16,4,128]{3,2,1,0:T(4,128)S(1)}, u32[]{:S(2)}) copy-start(f32[16,16,4,128]{3,2,1,0:T(4,128)S(1)} %reshape.345) | copy-start | bytes 1572868
  12.7 23.7 %copy-start.5 = (f32[16,4,256]{2,1,0:T(4,128)}, f32[16,4,256]{2,1,0:T(4,128)S(1)}, u32[]{:S(2)}) copy-start(f32[16,4,256]{2,1,0:T(4,128)S(1)} %fusion.12) | copy-start | bytes 196612
  16.6 22.0 %copy-start.18 = (f32[128]{0:T(128)S(1)}, f32[128]{0:T(128)}, u32[]{:S(2)}) copy-start(f32[128]{0:T(128)} %param.27) | copy-start | bytes 1540
  18.9 30.0 %all-to-all-start = ((f32[64,1,1024]{2,1,0:T(1,128)}), f32[64,1,1024]{2,1,0:T(1,128)S(1)}, u32[]{:S(2)}, u32[]{:S(2)}) async-start(f32[64,1,1024]{2,1,0:T(1,128)} %reshape.367), calls=%async_computation | async-start | bytes 524288 | tf_op jit(solution)/shard_map/all_to_all | solution.py:13
  52.2 0.8 copy-start.6
  52.3 0.8 copy-start.13
  56.0 7.6 %copy-start.4 = (f32[16,16,4,128]{3,2,1,0:T(4,128)S(1)}, f32[16,16,4,128]{3,2,1,0:T(4,128)}, u32[]{:S(2)}) copy-start(f32[16,16,4,128]{3,2,1,0:T(4,128)} %copy-done.3) | copy-start | bytes 1572868
  56.0 7.6 %copy-start.9 = (bf16[256,128]{1,0:T(8,128)(2,1)S(1)}, bf16[256,128]{1,0:T(8,128)(2,1)}, u32[]{:S(2)}) copy-start(bf16[256,128]{1,0:T(8,128)(2,1)} %multiply_convert_fusion) | copy-start | bytes 196612
  56.0 7.6 %copy-start.11 = (f32[16,16,4]{1,2,0:T(4,128)S(1)}, f32[16,16,4]{1,2,0:T(4,128)}, u32[]{:S(2)}) copy-start(f32[16,16,4]{1,2,0:T(4,128)} %copy-done.10) | copy-start | bytes 12292
  56.0 7.6 %copy-start.24 = (f32[128]{0:T(128)S(1)}, f32[128]{0:T(128)}, u32[]{:S(2)}) copy-start(f32[128]{0:T(128)} %param.26) | copy-start | bytes 1540
  57.9 21.4 %all-to-all-start.1 = ((bf16[64,4,4,129]{3,1,2,0:T(4,128)(2,1)}), bf16[64,4,4,129]{3,1,2,0:T(4,128)(2,1)S(1)}, u32[]{:S(2)}, u32[]{:S(2)}) async-start(bf16[64,4,4,129]{3,1,2,0:T(4,128)(2,1)} %copy.171), calls=%async_computation.1 | async-start | bytes 1048576 | tf_op jit(solution)/shard_map/all_to_all | solution.py:29
  (3 other events, 2.4 us)
where the time goes:
time: 109 us; the launch traced here: 108 us
  blocking collectives  26.9 us (25%)
  starting transfers between devices  23 us (21%)
  waiting for transfers between devices  21.3 us (20%)
  matrix products  13.2 us (12%)
  other arithmetic  12.1 us (11%)
  local copies, waits for them, and re-layouts  11 us (10%)
    all_to_all x1, blocking collectives, copy_for_each(): lax.all_to_all(jnp.broadcast_to(shard[None], (size, *shard.shape)), axis,...  19.9 us
    all_to_all x1, starting transfers between devices, copy_for_each(): lax.all_to_all(jnp.broadcast_to(shard[None], (size, *shard.shape)), axis,...  17.3 us
    all_to_all x1, waiting for transfers between devices, summed_on_arrival(): blocks = lax.all_to_all(in_blocks(shard, dim, size), axis, 0, 0, tiled=True)  12.7 us
    all_to_all x1, waiting for transfers between devices, copy_for_each(): lax.all_to_all(jnp.broadcast_to(shard[None], (size, *shard.shape)), axis,...  8.62 us
    all_to_all x1, blocking collectives, summed_on_arrival(): blocks = lax.all_to_all(in_blocks(shard, dim, size), axis, 0, 0, tiled=True)  6.95 us
    unnamed x55, local copies, waits for them, and re-layouts  6.08 us
    all_to_all x1, starting transfers between devices, summed_on_arrival(): blocks = lax.all_to_all(in_blocks(shard, dim, size), axis, 0, 0, tiled=True)  5.67 us
    dot_general x1, matrix products, shards(): jnp.einsum('spkgd,slkd->skgpl', queries, merged_keys, preferred_element_t...  3.03 us
  transfers between devices with their start and end apart: 2, of which 2 were waited for; matrix products, arithmetic and copies ran while one was open for 6% of the time, Pallas kernels for 0%

commit v1 on v0

v1 whole, which is shorter than its diff:
```python
import functools

import jax
import jax.numpy as jnp
from jax import lax
from jax.experimental import pallas as pl
from jax.experimental.pallas import tpu as pltpu
from jax.sharding import PartitionSpec as P

EPSILON = 1e-06
NEG_LARGE = -1e30
NEG_FLOOR = -1e29
HIGHEST = lax.Precision.HIGHEST
MESH = pl.DeviceIdType.MESH
F32 = jnp.float32
BF16 = jnp.bfloat16
LAST = (((1,), (1,)), ((), ()))


def iota(shape, dim):
    return lax.broadcasted_iota(jnp.int32, shape, dim)


def dot_last(a, b):
    return lax.dot_general(a, b, LAST, preferred_element_type=F32)


def unit(rows, gain):
    return rows * lax.rsqrt(jnp.mean(rows * rows, axis=-1, keepdims=True) + EPSILON) * gain


def kernel(
    seqs,
    heads,
    props,
    head,
    taken,
    block,
    tokens_hbm,
    norm_gain,
    query_hbm,
    key_hbm,
    value_hbm,
    forget,
    forget_bias,
    query_gain,
    key_gain,
    out_weight,
    keys_hbm,
    values_hbm,
    logcum,
    pending_keys,
    pending_values,
    pending_logcum,
    lengths,
    accepted,
    accepted_row,
    parents,
    result,
    tok,
    normed,
    wq,
    wk,
    wv,
    kbuf,
    vbuf,
    q_scr,
    kn_scr,
    vn_scr,
    anc_scr,
    cum_scr,
    o_send,
    o_recv,
    lse_send,
    lse_recv,
    tree_scr,
    att,
    swap_send,
    swap_recv,
    load_sem,
    send_sem,
    recv_sem,
):
    rows = seqs * props
    peers = seqs * heads
    scaling = head**-0.5
    me = lax.axis_index("kv")
    core = lax.axis_index("tp")
    my_seq = me // heads
    my_head = me % heads

    def load(src, dst, n):
        return pltpu.make_async_copy(src, dst, load_sem.at[n])

    loads = [
        load(tokens_hbm, tok, 0),
        load(key_hbm, wk, 1),
        load(value_hbm, wv, 2),
        load(query_hbm, wq, 3),
        load(keys_hbm, kbuf, 4),
        load(values_hbm, vbuf, 5),
    ]
    for item in loads:
        item.start()

    barrier = pltpu.get_barrier_semaphore()

    @pl.loop(1, peers)
    def _(step):
        pl.semaphore_signal(
            barrier, inc=1, device_id={"kv": (me + step) % peers}, device_id_type=MESH
        )

    pl.semaphore_signal(barrier, inc=1, device_id={"tp": 1 - core}, device_id_type=MESH)

    lane = iota((seqs, rows), 1)
    spread = ((iota((props, rows), 1) & (props - 1)) == iota((props, rows), 0)).astype(BF16)
    repeated = jnp.dot(
        parents[...].astype(F32).astype(BF16), spread, preferred_element_type=F32
    )
    parent_row = jnp.sum(
        jnp.where(lane // props == iota((seqs, rows), 0), repeated, 0.0), axis=0, keepdims=True
    ).astype(jnp.int32)
    down = iota((rows, rows), 0)
    across = iota((rows, rows), 1)
    same = down // props == across // props
    linked = (same & (parent_row == (down & (props - 1)))) | (down == across)
    anc_t = jnp.where(linked, 1.0, 0.0).astype(BF16)
    for _ in range((props - 1).bit_length()):
        anc_t = jnp.minimum(jnp.dot(anc_t, anc_t, preferred_element_type=F32), 1.0).astype(BF16)
    anc_scr[...] = anc_t

    loads[0].wait()

    @pl.loop(0, rows // 16)
    def _(step):
        piece = pl.ds(step * 16, 16)
        wide = tok[piece, :].astype(F32)
        normed[piece, :] = unit(wide, norm_gain[...]).astype(BF16)

    gate_raw = dot_last(forget[...], normed[...])
    gate_head = iota((2 * heads, 1), 0)
    bias = jnp.zeros((2 * heads, 1), F32)
    for n in range(2 * heads):
        bias = jnp.where(gate_head == n, forget_bias[n], bias)
    gate_raw = gate_raw + bias
    gates = jnp.minimum(gate_raw, 0.0) - jnp.log1p(jnp.exp(-jnp.abs(gate_raw)))
    gates = jnp.where(
        core == 0, gates, jnp.concatenate([gates[heads:], gates[:heads]], axis=0)
    )
    base = jnp.zeros((heads, seqs), F32)
    for a in range(taken):
        base = jnp.where(accepted_row[...] - 1 == a, pending_logcum[a], base)
    base = jnp.concatenate([base, jnp.zeros((heads, seqs), F32)], axis=0)
    expand = (lane // props == iota((seqs, rows), 0)).astype(F32)
    cum_t = jnp.dot(
        gates, anc_t.astype(F32), precision=HIGHEST, preferred_element_type=F32
    ) + jnp.dot(base, expand, precision=HIGHEST, preferred_element_type=F32)
    cum_scr[...] = cum_t.T

    loads[1].wait()
    kn_scr[...] = unit(
        jnp.dot(normed[...], wk[...], preferred_element_type=F32), key_gain[...]
    ).astype(BF16)
    loads[2].wait()
    vn_scr[...] = jnp.dot(normed[...], wv[...], preferred_element_type=F32).astype(BF16)
    loads[3].wait()
    for h in range(heads):
        raw = jnp.dot(
            normed[...], wq[:, h * head : (h + 1) * head], preferred_element_type=F32
        )
        q_scr[:, h * props : (h + 1) * props, :] = (
            unit(raw, query_gain[...]).astype(BF16).reshape(seqs, props, head)
        )

    o_recv[pl.ds(peers, 8)] = jnp.zeros((8, props, head), BF16)
    lse_recv[pl.ds(peers, 8)] = jnp.full((8, 1, 128), NEG_LARGE, F32)

    loads[4].wait()
    loads[5].wait()
    pl.semaphore_wait(barrier, peers)

    def send_out(k):
        return pltpu.make_async_remote_copy(
            src_ref=o_send.at[k],
            dst_ref=o_recv.at[me],
            send_sem=send_sem.at[0],
            recv_sem=recv_sem.at[0],
            device_id={"kv": k},
            device_id_type=MESH,
        )

    def send_lse(k):
        return pltpu.make_async_remote_copy(
            src_ref=lse_send.at[k // heads],
            dst_ref=lse_recv.at[me],
            send_sem=send_sem.at[1],
            recv_sem=recv_sem.at[1],
            device_id={"kv": k},
            device_id_type=MESH,
        )

    def send_att(k):
        mine = att.at[my_head * seqs + my_seq]
        return pltpu.make_async_remote_copy(
            src_ref=mine,
            dst_ref=mine,
            send_sem=send_sem.at[2],
            recv_sem=recv_sem.at[2],
            device_id={"kv": k},
            device_id_type=MESH,
        )

    def all_but_one(ref, n):
        some = ref.at[pl.ds(0, peers - 1)]
        return pltpu.make_async_remote_copy(
            src_ref=some,
            dst_ref=some,
            send_sem=send_sem.at[n],
            recv_sem=recv_sem.at[n],
            device_id={"kv": me},
            device_id_type=MESH,
        )

    planes = seqs // 2
    my_plane = my_seq // 2
    place = me * block + iota((1, block), 1)

    @pl.loop(0, planes // 2, init_carry=jnp.zeros((heads * props, 128), F32))
    def lse_cols(g, cols):
        members = []
        for far in (planes // 2 + g, planes // 2 - 1 - g):
            plane = (my_plane + far) % planes
            members += [2 * plane, 2 * plane + 1]
        for s in members:
            raw = dot_last(q_scr[s], kbuf[s])
            minus = jnp.where(place < lengths[s], -logcum[s], NEG_LARGE)
            cum = cum_scr[pl.ds(pl.multiple_of(s * props, props), props), :]
            scores = jnp.concatenate(
                [
                    raw[h * props : (h + 1) * props] * scaling
                    + (cum[:, h : h + 1] + minus[h : h + 1])
                    for h in range(heads)
                ],
                axis=0,
            )
            top = jnp.maximum(jnp.max(scores, axis=-1, keepdims=True), NEG_FLOOR)
            weights = jnp.exp(scores - top)
            total = jnp.sum(weights, axis=-1, keepdims=True)
            some = total > 0.0
            safe = jnp.where(some, total, 1.0)
            out = jnp.dot(weights.astype(BF16), vbuf[s], preferred_element_type=F32)
            out = (out * (1.0 / safe)).astype(BF16)
            o_send[pl.ds(s * heads, heads)] = out.reshape(heads, props, head)
            lse = jnp.where(some, top + jnp.log(safe), NEG_LARGE)
            cols = jnp.where(iota((heads * props, 128), 1) == s, lse, cols)
        for s in members:
            for h in range(heads):
                k = s * heads + h

                @pl.when(k != me)
                def _():
                    send_out(k).start()

                @pl.when(k == me)
                def _():
                    o_recv[me] = o_send[k]

        return cols

    padded = jnp.concatenate([lse_cols, jnp.zeros((128 - heads * props, 128), F32)], axis=0)
    lse_rows = padded.T
    for s in range(seqs):
        lse_send[s] = lse_rows[s : s + 1]
    lse_recv[me] = lse_send[my_seq]

    @pl.loop(1, peers)
    def _(step):
        send_lse((me + step) % peers).start()

    width = heads * props
    q_own = q_scr[my_seq]
    own_rows = pl.ds(pl.multiple_of(my_seq * props, props), props)
    extra = 16
    pad = jnp.zeros((extra - taken, head), F32)
    keys_x = jnp.concatenate(
        [
            kn_scr[own_rows, :].astype(F32),
            pending_keys[my_seq].astype(F32),
            pad,
        ],
        axis=0,
    ).astype(BF16)
    values_x = jnp.concatenate(
        [
            vn_scr[own_rows, :].astype(F32),
            pending_values[my_seq].astype(F32),
            pad,
        ],
        axis=0,
    ).astype(BF16)
    raw_t = dot_last(keys_x, q_own)
    cum_own = cum_scr[own_rows, :]
    lane_head = iota((props, width), 1) // props
    lane_prop = iota((props, width), 1) & (props - 1)
    cum_wide = jnp.zeros((props, width), F32)
    for h in range(heads):
        cum_wide = jnp.where(lane_head == h, cum_own[:, h : h + 1], cum_wide)
    cum_row = jnp.sum(
        jnp.where(lane_prop == iota((props, width), 0), cum_wide, 0.0), axis=0, keepdims=True
    )
    anc_fold = (
        (iota((rows, width), 0) & (props - 1)) == (iota((rows, width), 1) & (props - 1))
    ).astype(BF16)
    anc_own = jnp.dot(anc_scr[own_rows, :], anc_fold, preferred_element_type=F32)
    pend_wide = jnp.zeros((extra, width), F32)
    pend_sub = iota((extra, width), 0)
    for a in range(taken):
        col = jnp.sum(
            jnp.where(iota((heads, seqs), 1) == my_seq, pending_logcum[a], 0.0),
            axis=1,
            keepdims=True,
        )
        row = jnp.sum(
            jnp.where(iota((heads, width), 1) // props == iota((heads, width), 0), col, 0.0),
            axis=0,
            keepdims=True,
        )
        pend_wide = jnp.where(pend_sub == a, row, pend_wide)
    tree_t = jnp.where(
        anc_own > 0.5, raw_t[:props] * scaling + cum_row - cum_wide, NEG_LARGE
    )
    pend_t = jnp.where(
        pend_sub < accepted[my_seq], raw_t[props:] * scaling + cum_row - pend_wide, NEG_LARGE
    )
    both_t = jnp.concatenate([tree_t, pend_t], axis=0)
    top_t = jnp.max(both_t, axis=0, keepdims=True)
    weights_t = jnp.exp(both_t - top_t)
    total_t = jnp.sum(weights_t, axis=0, keepdims=True)
    share_t = (weights_t * (1.0 / total_t)).astype(BF16)
    tree_scr[...] = lax.dot_general(
        share_t, values_x, (((0,), (0,)), ((), ())), preferred_element_type=F32
    )
    head_rows = pl.ds(pl.multiple_of(my_head * props, props), props)
    o_recv[peers] = tree_scr[head_rows, :].astype(BF16)
    lse_t = top_t + jnp.log(total_t)
    lse_recv[peers] = jnp.concatenate([lse_t, jnp.zeros((1, 128 - width), F32)], axis=1)

    all_but_one(lse_recv, 1).wait_recv()
    slots = peers + 8
    lse_all = lse_recv[:, 0, :]
    weight = jnp.exp(lse_all - jnp.max(lse_all, axis=0, keepdims=True)).astype(BF16)
    pick = (
        (iota((128, 128), 0) - my_head * props) == (iota((128, 128), 1) & (props - 1))
    ).astype(BF16)
    picked = jnp.dot(weight, pick, preferred_element_type=F32)
    mine_8 = iota((8, 128), 1) // props == iota((8, 128), 0)
    mine_16 = (iota((props, 128), 1) & (props - 1)) == iota((props, 128), 0)
    mixes = []
    for c in range(slots // 8):
        flat = jnp.sum(
            jnp.where(mine_8, picked[c * 8 : (c + 1) * 8], 0.0), axis=0, keepdims=True
        )
        mixes.append(jnp.where(mine_16, flat, 0.0))
    den = functools.reduce(lambda a, b: a + b, mixes)
    den = jnp.sum(den, axis=1, keepdims=True)
    mix = jnp.concatenate(mixes, axis=1).astype(BF16)
    all_but_one(o_recv, 0).wait_recv()
    blended = jnp.dot(
        mix, o_recv[...].reshape(slots * props, head), preferred_element_type=F32
    )
    att[my_head * seqs + my_seq] = (blended / den).astype(BF16)

    @pl.loop(1, peers)
    def _(step):
        send_att((me + step) % peers).start()

    all_but_one(att, 2).wait_recv()

    part_t = jnp.zeros((out_weight.shape[0], rows), F32)
    for h in range(heads):
        part_t += dot_last(
            out_weight[:, h * head : (h + 1) * head],
            att[pl.ds(h * seqs, seqs)].reshape(rows, head),
        )
    half = out_weight.shape[0] // 2
    low, high = part_t[:half].astype(BF16), part_t[half:].astype(BF16)
    swap_send[...] = jnp.where(core == 0, high, low)
    swap = pltpu.make_async_remote_copy(
        src_ref=swap_send,
        dst_ref=swap_recv,
        send_sem=send_sem.at[3],
        recv_sem=recv_sem.at[3],
        device_id={"tp": 1 - core},
        device_id_type=MESH,
    )
    swap.start()
    kept = jnp.where(core == 0, low, high).astype(F32)
    swap.wait()
    final = kept + swap_recv[...].astype(F32)
    result[...] = final.T.astype(BF16).reshape(seqs, props, half)

    all_but_one(o_send, 0).wait_send()
    all_but_one(lse_recv, 1).wait_send()
    all_but_one(att, 2).wait_send()


def shards(
    tokens,
    norm_gain,
    query_weight,
    key_weight,
    value_weight,
    forget_weight,
    forget_bias,
    query_gain,
    key_gain,
    output_weight,
    cache_keys,
    cache_values,
    cache_logcum,
    pending_keys,
    pending_values,
    pending_logcum,
    lengths,
    accepted,
    parents,
):
    seqs, props, width = tokens.shape
    head = query_gain.shape[0]
    heads = query_weight.shape[1] // head
    block = cache_keys.shape[1]
    taken = pending_keys.shape[1]
    rows = seqs * props
    peers = seqs * heads
    half = output_weight.shape[1] // 2
    whole = pl.BlockSpec(memory_space=pltpu.VMEM)
    scalars = pl.BlockSpec(memory_space=pltpu.SMEM)
    stay = pl.BlockSpec(memory_space=pl.ANY)
    operands = [
        (tokens.reshape(rows, width), stay),
        (norm_gain.reshape(1, width), whole),
        (query_weight, stay),
        (key_weight, stay),
        (value_weight, stay),
        (forget_weight.T, whole),
        (forget_bias, scalars),
        (query_gain.reshape(1, head), whole),
        (key_gain.reshape(1, head), whole),
        (output_weight.T, whole),
        (cache_keys.reshape(seqs, block, head), stay),
        (cache_values.reshape(seqs, block, head), stay),
        (jnp.swapaxes(cache_logcum, 1, 2), whole),
        (pending_keys.reshape(seqs, taken, head), whole),
        (pending_values.reshape(seqs, taken, head), whole),
        (jnp.transpose(pending_logcum, (1, 2, 0)), whole),
        (lengths, scalars),
        (accepted, scalars),
        (accepted.reshape(1, seqs), whole),
        (parents, whole),
    ]
    return pl.pallas_call(
        functools.partial(kernel, seqs, heads, props, head, taken, block),
        out_shape=jax.ShapeDtypeStruct((seqs, props, half), BF16),
        in_specs=[spec for _, spec in operands],
        out_specs=whole,
        scratch_shapes=[
            pltpu.VMEM((rows, width), BF16),
            pltpu.VMEM((rows, width), BF16),
            pltpu.VMEM((width, heads * head), BF16),
            pltpu.VMEM((width, head), BF16),
            pltpu.VMEM((width, head), BF16),
            pltpu.VMEM((seqs, block, head), BF16),
            pltpu.VMEM((seqs, block, head), BF16),
            pltpu.VMEM((seqs, heads * props, head), BF16),
            pltpu.VMEM((rows, head), BF16),
            pltpu.VMEM((rows, head), BF16),
            pltpu.VMEM((rows, rows), BF16),
            pltpu.VMEM((rows, 2 * heads), F32),
            pltpu.VMEM((peers, props, head), BF16),
            pltpu.VMEM((peers + 8, props, head), BF16),
            pltpu.VMEM((seqs, 1, 128), F32),
            pltpu.VMEM((peers + 8, 1, 128), F32),
            pltpu.VMEM((heads * props, head), F32),
            pltpu.VMEM((peers, props, head), BF16),
            pltpu.VMEM((half, rows), BF16),
            pltpu.VMEM((half, rows), BF16),
            pltpu.SemaphoreType.DMA((6,)),
            pltpu.SemaphoreType.DMA((4,)),
            pltpu.SemaphoreType.DMA((4,)),
        ],
        compiler_params=pltpu.CompilerParams(
            collective_id=0, has_side_effects=True, vmem_limit_bytes=48 * 1024 * 1024
        ),
    )(*[array for array, _ in operands])


def solution(mesh):
    placed = (
        P("dp", None, None),
        P(),
        P(None, "tp"),
        P(None, "tp"),
        P(None, "tp"),
        P(),
        P(),
        P(),
        P(),
        P("tp", "kv"),
        P("dp", "kv", "tp", None),
        P("dp", "kv", "tp", None),
        P("dp", "kv", "tp"),
        P("dp", None, "tp", None),
        P("dp", None, "tp", None),
        P("dp", None, "tp"),
        P("dp"),
        P("dp"),
        P("dp", None),
    )
    return jax.shard_map(
        shards, mesh=mesh, in_specs=placed, out_specs=P("dp", None, ("kv", "tp")), check_vma=False
    )
```

time: 109 us -> 59.7 us (0.55)
  Pallas kernels: 0 us -> 43.4 us
  blocking collectives: 26.9 us -> 0 us
  starting transfers between devices: 23 us -> 0 us
  waiting for transfers between devices: 21.3 us -> 0 us
  matrix products: 13.2 us -> 0 us
  other arithmetic: 12.1 us -> 0 us
  local copies, waits for them, and re-layouts: 11 us -> 15.5 us
    pallas_call x0 -> x1, Pallas kernels: none -> 43.4 us  [shards(): pl.pallas_call(functools.partial(kernel, seqs, heads, props, head, taken,...]
    all_to_all x2 -> x0, blocking collectives: 26.9 us -> none  [the longest x1 19.9 us: copy_for_each(): lax.all_to_all(jnp.broadcast_to(shard[None], (size, *shard.shape)), axis,...]
    all_to_all x2 -> x0, starting transfers between devices: 23 us -> none  [the longest x1 17.3 us: copy_for_each(): lax.all_to_all(jnp.broadcast_to(shard[None], (size, *shard.shape)), axis,...]
    all_to_all x2 -> x0, waiting for transfers between devices: 21.3 us -> none  [the longest x1 12.7 us: summed_on_arrival(): blocks = lax.all_to_all(in_blocks(shard, dim, size), axis, 0, 0, tiled=True)]
    dot_general x14 -> x0, matrix products: 13.2 us -> none  [the longest x1 3.03 us: shards(): jnp.einsum('spkgd,slkd->skgpl', queries, merged_keys, preferred_element_t...]
    unnamed x55 -> x37, local copies, waits for them, and re-layouts: 6.08 us -> 15.5 us
    reduce_sum x7 -> x0, other arithmetic: 5.28 us -> none  [the longest x1 1.49 us: shards(): jnp.mean(widened * widened, axis=-1, keepdims=True) + EPSILON]
    convert_element_type x4 -> x0, other arithmetic: 1.97 us -> none  [the longest x1 1.64 us: shards(): key_part.astype(jnp.bfloat16)]
  transfers between devices with their start and end apart: 2 -> 0, of which waited for: 2 -> 0; matrix products, arithmetic and copies ran while one was open for 6% -> 0% of each run, Pallas kernels for 0% -> 0%
where the time goes in v1:
time: 59.7 us; the launch traced here: 59 us
  Pallas kernels  43.4 us (73%)
  local copies, waits for them, and re-layouts  15.5 us (26%)
    pallas_call x1, Pallas kernels, shards(): pl.pallas_call(functools.partial(kernel, seqs, heads, props, head, taken,...  43.4 us
    unnamed x37, local copies, waits for them, and re-layouts  15.5 us

profile of v1, /device:TPU:1, one launch (start us, length us, event | category | flops | bytes accessed | tf_op | source)
XLA Modules:
  0.0 59.0 jit_solution(14844694938769231509)
XLA Ops:
  0.0 0.0 copy-start
  0.0 1.2 %copy-done = bf16[16,16,2048]{2,1,0:T(8,128)(2,1)S(1)} copy-done((bf16[16,16,2048]{2,1,0:T(8,128)(2,1)S(1)}, bf16[16,16,2048]{2,1,0:T(8,128)(2,1)}, u32[]{:S(2)}) %copy-start) | copy-done | bytes 1048600
  1.2 0.0 copy-start.1
  1.2 1.2 %copy-done.1 = bf16[16,256,1,128]{3,1,2,0:T(8,128)(2,1)S(1)} copy-done((bf16[16,256,1,128]{3,1,2,0:T(8,128)(2,1)S(1)}, bf16[16,256,1,128]{3,1,2,0:T(8,128)(2,1)}, u32[]{:S(2)}) %copy-start.1) | copy-done | bytes 1048600
  2.5 0.0 copy-start.2
  2.5 1.2 %copy-done.2 = bf16[16,256,1,128]{3,1,2,0:T(8,128)(2,1)S(1)} copy-done((bf16[16,256,1,128]{3,1,2,0:T(8,128)(2,1)S(1)}, bf16[16,256,1,128]{3,1,2,0:T(8,128)(2,1)}, u32[]{:S(2)}) %copy-start.2) | copy-done | bytes 1048600
  3.7 0.0 copy-start.3
  3.7 1.0 %copy-done.3 = bf16[2048,128]{1,0:T(8,128)(2,1)S(1)} copy-done((bf16[2048,128]{1,0:T(8,128)(2,1)S(1)}, bf16[2048,128]{1,0:T(8,128)(2,1)}, u32[]{:S(2)}) %copy-start.3) | copy-done | bytes 524312
  4.7 1.0 %copy-done.4 = bf16[2048,128]{1,0:T(8,128)(2,1)S(1)} copy-done((bf16[2048,128]{1,0:T(8,128)(2,1)S(1)}, bf16[2048,128]{1,0:T(8,128)(2,1)}, u32[]{:S(2)}) %copy-start.4) | copy-done | bytes 524312
  5.8 0.8 %copy-done.5 = f32[16,256,4]{1,2,0:T(4,128)S(1)} copy-done((f32[16,256,4]{1,2,0:T(4,128)S(1)}, f32[16,256,4]{1,2,0:T(4,128)}, u32[]{:S(2)}) %copy-start.5) | copy-done | bytes 65560
  6.6 0.8 %copy-done.6 = bf16[2048,8]{0,1:T(8,128)(2,1)S(1)} copy-done((bf16[2048,8]{0,1:T(8,128)(2,1)S(1)}, bf16[2048,8]{0,1:T(8,128)(2,1)}, u32[]{:S(2)}) %copy-start.6) | copy-done | bytes 32792
  7.4 0.8 %copy-done.7 = bf16[512,32]{0,1:T(8,128)(2,1)S(1)} copy-done((bf16[512,32]{0,1:T(8,128)(2,1)S(1)}, bf16[512,32]{0,1:T(8,128)(2,1)}, u32[]{:S(2)}) %copy-start.7) | copy-done | bytes 32792
  8.1 0.7 %copy-done.8 = bf16[16,4,1,128]{3,1,2,0:T(4,128)(2,1)S(1)} copy-done((bf16[16,4,1,128]{3,1,2,0:T(4,128)(2,1)S(1)}, bf16[16,4,1,128]{3,1,2,0:T(4,128)(2,1)}, u32[]{:S(2)}) %copy-start.8) | copy-done | bytes 16408
  8.8 0.7 %copy-done.9 = bf16[16,4,1,128]{3,1,2,0:T(4,128)(2,1)S(1)} copy-done((bf16[16,4,1,128]{3,1,2,0:T(4,128)(2,1)S(1)}, bf16[16,4,1,128]{3,1,2,0:T(4,128)(2,1)}, u32[]{:S(2)}) %copy-start.9) | copy-done | bytes 16408
  9.6 0.7 %copy-done.10 = f32[2048]{0:T(1024)S(1)} copy-done((f32[2048]{0:T(1024)S(1)}, f32[2048]{0:T(1024)}, u32[]{:S(2)}) %copy-start.10) | copy-done | bytes 8216
  10.3 0.7 %copy-done.11 = f32[16,4,4]{0,2,1:T(4,128)S(1)} copy-done((f32[16,4,4]{0,2,1:T(4,128)S(1)}, f32[16,4,4]{0,2,1:T(4,128)}, u32[]{:S(2)}) %copy-start.11) | copy-done | bytes 1048
  10.9 0.7 %copy-done.12 = s32[16,16]{1,0:T(8,128)S(1)} copy-done((s32[16,16]{1,0:T(8,128)S(1)}, s32[16,16]{1,0:T(8,128)}, u32[]{:S(2)}) %copy-start.12) | copy-done | bytes 1048
  11.6 0.7 %copy-done.13 = s32[16]{0:T(128)S(1)} copy-done((s32[16]{0:T(128)S(1)}, s32[16]{0:T(128)}, u32[]{:S(2)}) %copy-start.13) | copy-done | bytes 88
  12.3 0.7 %copy-done.14 = f32[8]{0:T(128)S(1)} copy-done((f32[8]{0:T(128)S(1)}, f32[8]{0:T(128)}, u32[]{:S(2)}) %copy-start.14) | copy-done | bytes 56
  13.0 0.7 %copy-done.15 = f32[128]{0:T(128)S(1)} copy-done((f32[128]{0:T(128)S(1)}, f32[128]{0:T(128)}, u32[]{:S(2)}) %copy-start.15) | copy-done | bytes 536
  13.6 0.7 %copy-done.16 = f32[128]{0:T(128)S(1)} copy-done((f32[128]{0:T(128)S(1)}, f32[128]{0:T(128)}, u32[]{:S(2)}) %copy-start.16) | copy-done | bytes 536
  14.3 0.7 %copy-done.17 = s32[16]{0:T(128)S(1)} copy-done((s32[16]{0:T(128)S(1)}, s32[16]{0:T(128)}, u32[]{:S(2)}) %copy-start.17) | copy-done | bytes 88
  14.9 43.4 %shard_map.181 = bf16[16,16,16]{2,1,0:T(8,128)(2,1)S(1)} custom-call(bf16[256,2048]{1,0:T(8,128)(2,1)S(1)} %bitcast.13, f32[1,2048]{1,0:T(1,128)S(1)} %bitcast.21, bf16[2048,512]{1,0:T(8,128)(2,1)} %query_hbm.1, bf16[2048,128]{1,0:T(8,128)(2,1)S(1)} %copy-done.3, bf16[2048,128]{1,0:T(8,128)(2,1)S(1)} %copy-done.4, bf16[8,2048]{1,0:T(8,128)(2,1)S(1)} %bitcast.17, ...), custom_call_target="tpu_custom_call" | custom-call | tf_op jit(solution)/shard_map/pallas_call | solution.py:462
  58.3 0.6 %copy.21 = bf16[16,16,16]{2,1,0:T(8,128)(2,1)} copy(bf16[16,16,16]{2,1,0:T(8,128)(2,1)S(1)} %shard_map.181) | data formatting | bytes 16384
  (14 shorter events, 0.0 us)
Async XLA Ops:
  0.0 1.2 %copy-start = (bf16[16,16,2048]{2,1,0:T(8,128)(2,1)S(1)}, bf16[16,16,2048]{2,1,0:T(8,128)(2,1)}, u32[]{:S(2)}) copy-start(bf16[16,16,2048]{2,1,0:T(8,128)(2,1)} %param.19) | copy-start | bytes 3145732
  1.2 1.2 %copy-start.1 = (bf16[16,256,1,128]{3,1,2,0:T(8,128)(2,1)S(1)}, bf16[16,256,1,128]{3,1,2,0:T(8,128)(2,1)}, u32[]{:S(2)}) copy-start(bf16[16,256,1,128]{3,1,2,0:T(8,128)(2,1)} %param.29) | copy-start | bytes 3145732
  2.5 1.2 %copy-start.2 = (bf16[16,256,1,128]{3,1,2,0:T(8,128)(2,1)S(1)}, bf16[16,256,1,128]{3,1,2,0:T(8,128)(2,1)}, u32[]{:S(2)}) copy-start(bf16[16,256,1,128]{3,1,2,0:T(8,128)(2,1)} %param.30) | copy-start | bytes 3145732
  3.7 1.0 %copy-start.3 = (bf16[2048,128]{1,0:T(8,128)(2,1)S(1)}, bf16[2048,128]{1,0:T(8,128)(2,1)}, u32[]{:S(2)}) copy-start(bf16[2048,128]{1,0:T(8,128)(2,1)} %key_hbm.1) | copy-start | bytes 1572868
  4.7 1.0 %copy-start.4 = (bf16[2048,128]{1,0:T(8,128)(2,1)S(1)}, bf16[2048,128]{1,0:T(8,128)(2,1)}, u32[]{:S(2)}) copy-start(bf16[2048,128]{1,0:T(8,128)(2,1)} %value_hbm.1) | copy-start | bytes 1572868
  5.8 0.8 %copy-start.5 = (f32[16,256,4]{1,2,0:T(4,128)S(1)}, f32[16,256,4]{1,2,0:T(4,128)}, u32[]{:S(2)}) copy-start(f32[16,256,4]{1,2,0:T(4,128)} %param.31) | copy-start | bytes 196612
  6.6 0.8 %copy-start.6 = (bf16[2048,8]{0,1:T(8,128)(2,1)S(1)}, bf16[2048,8]{0,1:T(8,128)(2,1)}, u32[]{:S(2)}) copy-start(bf16[2048,8]{0,1:T(8,128)(2,1)} %param.24) | copy-start | bytes 98308
  7.4 0.8 %copy-start.7 = (bf16[512,32]{0,1:T(8,128)(2,1)S(1)}, bf16[512,32]{0,1:T(8,128)(2,1)}, u32[]{:S(2)}) copy-start(bf16[512,32]{0,1:T(8,128)(2,1)} %param.28) | copy-start | bytes 98308
  8.1 0.7 %copy-start.8 = (bf16[16,4,1,128]{3,1,2,0:T(4,128)(2,1)S(1)}, bf16[16,4,1,128]{3,1,2,0:T(4,128)(2,1)}, u32[]{:S(2)}) copy-start(bf16[16,4,1,128]{3,1,2,0:T(4,128)(2,1)} %param.32) | copy-start | bytes 49156
  8.8 0.7 %copy-start.9 = (bf16[16,4,1,128]{3,1,2,0:T(4,128)(2,1)S(1)}, bf16[16,4,1,128]{3,1,2,0:T(4,128)(2,1)}, u32[]{:S(2)}) copy-start(bf16[16,4,1,128]{3,1,2,0:T(4,128)(2,1)} %param.33) | copy-start | bytes 49156
  9.6 0.7 %copy-start.10 = (f32[2048]{0:T(1024)S(1)}, f32[2048]{0:T(1024)}, u32[]{:S(2)}) copy-start(f32[2048]{0:T(1024)} %param.20) | copy-start | bytes 24580
  10.3 0.7 %copy-start.11 = (f32[16,4,4]{0,2,1:T(4,128)S(1)}, f32[16,4,4]{0,2,1:T(4,128)}, u32[]{:S(2)}) copy-start(f32[16,4,4]{0,2,1:T(4,128)} %param.34) | copy-start | bytes 3076
  10.9 0.7 %copy-start.12 = (s32[16,16]{1,0:T(8,128)S(1)}, s32[16,16]{1,0:T(8,128)}, u32[]{:S(2)}) copy-start(s32[16,16]{1,0:T(8,128)} %parents.1) | copy-start | bytes 3076
  11.6 0.7 %copy-start.13 = (s32[16]{0:T(128)S(1)}, s32[16]{0:T(128)}, u32[]{:S(2)}) copy-start(s32[16]{0:T(128)} %accepted.1) | copy-start | bytes 196
  12.3 0.7 %copy-start.14 = (f32[8]{0:T(128)S(1)}, f32[8]{0:T(128)}, u32[]{:S(2)}) copy-start(f32[8]{0:T(128)} %forget_bias.1) | copy-start | bytes 100
  13.0 0.7 %copy-start.15 = (f32[128]{0:T(128)S(1)}, f32[128]{0:T(128)}, u32[]{:S(2)}) copy-start(f32[128]{0:T(128)} %param.26) | copy-start | bytes 1540
  13.6 0.7 %copy-start.16 = (f32[128]{0:T(128)S(1)}, f32[128]{0:T(128)}, u32[]{:S(2)}) copy-start(f32[128]{0:T(128)} %param.27) | copy-start | bytes 1540
  14.3 0.7 %copy-start.17 = (s32[16]{0:T(128)S(1)}, s32[16]{0:T(128)}, u32[]{:S(2)}) copy-start(s32[16]{0:T(128)} %lengths.1) | copy-start | bytes 196

commit v2 on v1

--- a/solution.py
+++ b/solution.py
@@ -15,6 +15,51 @@
 F32 = jnp.float32
 BF16 = jnp.bfloat16
 LAST = (((1,), (1,)), ((), ()))
+NAMES = (
+    "tokens",
+    "norm_gain",
+    "query_weight",
+    "key_weight",
+    "value_weight",
+    "forget",
+    "forget_bias",
+    "query_gain",
+    "key_gain",
+    "out_weight",
+    "keys",
+    "values",
+    "logcum",
+    "pending_keys",
+    "pending_values",
+    "pending_logcum",
+    "lengths",
+    "accepted",
+    "accepted_row",
+    "parents",
+)
+SCALARS = ("forget_bias", "lengths", "accepted")
+LOAD_ORDER = (
+    "parents",
+    "tokens",
+    "norm_gain",
+    "forget",
+    "forget_bias",
+    "accepted_row",
+    "pending_logcum",
+    "key_gain",
+    "query_gain",
+    "key_weight",
+    "value_weight",
+    "query_weight",
+    "keys",
+    "logcum",
+    "lengths",
+    "values",
+    "accepted",
+    "pending_keys",
+    "pending_values",
+    "out_weight",
+)
 
 
 def iota(shape, dim):
@@ -36,34 +81,10 @@
     head,
     taken,
     block,
-    tokens_hbm,
-    norm_gain,
-    query_hbm,
-    key_hbm,
-    value_hbm,
-    forget,
-    forget_bias,
-    query_gain,
-    key_gain,
-    out_weight,
-    keys_hbm,
-    values_hbm,
-    logcum,
-    pending_keys,
-    pending_values,
-    pending_logcum,
-    lengths,
-    accepted,
-    accepted_row,
-    parents,
+    operands,
     result,
-    tok,
+    places,
     normed,
-    wq,
-    wk,
-    wv,
-    kbuf,
-    vbuf,
     q_scr,
     kn_scr,
     vn_scr,
@@ -89,19 +110,17 @@
     my_seq = me // heads
     my_head = me % heads
 
-    def load(src, dst, n):
-        return pltpu.make_async_copy(src, dst, load_sem.at[n])
-
-    loads = [
-        load(tokens_hbm, tok, 0),
-        load(key_hbm, wk, 1),
-        load(value_hbm, wv, 2),
-        load(query_hbm, wq, 3),
-        load(keys_hbm, kbuf, 4),
-        load(values_hbm, vbuf, 5),
-    ]
-    for item in loads:
+    loads = {
+        name: pltpu.make_async_copy(operands[name], places[name], load_sem.at[n])
+        for n, name in enumerate(LOAD_ORDER)
+    }
+    for item in loads.values():
         item.start()
+    (
+        tok, norm_gain, wq, wk, wv, forget, forget_bias, query_gain, key_gain, out_weight,
+        kbuf, vbuf, logcum, pending_keys, pending_values, pending_logcum, lengths, accepted,
+        accepted_row, parents,
+    ) = (places[name] for name in NAMES)
 
     barrier = pltpu.get_barrier_semaphore()
 
@@ -112,6 +131,8 @@
         )
 
     pl.semaphore_signal(barrier, inc=1, device_id={"tp": 1 - core}, device_id_type=MESH)
+
+    loads["parents"].wait()
 
     lane = iota((seqs, rows), 1)
     spread = ((iota((props, rows), 1) & (props - 1)) == iota((props, rows), 0)).astype(BF16)
@@ -130,7 +151,8 @@
         anc_t = jnp.minimum(jnp.dot(anc_t, anc_t, preferred_element_type=F32), 1.0).astype(BF16)
     anc_scr[...] = anc_t
 
-    loads[0].wait()
+    loads["tokens"].wait()
+    loads["norm_gain"].wait()
 
     @pl.loop(0, rows // 16)
     def _(step):
@@ -138,6 +160,8 @@
         wide = tok[piece, :].astype(F32)
         normed[piece, :] = unit(wide, norm_gain[...]).astype(BF16)
 
+    for name in ("forget", "forget_bias", "accepted_row", "pending_logcum"):
+        loads[name].wait()
     gate_raw = dot_last(forget[...], normed[...])
     gate_head = iota((2 * heads, 1), 0)
     bias = jnp.zeros((2 * heads, 1), F32)
@@ -158,13 +182,15 @@
     ) + jnp.dot(base, expand, precision=HIGHEST, preferred_element_type=F32)
     cum_scr[...] = cum_t.T
 
-    loads[1].wait()
+    loads["key_gain"].wait()
+    loads["key_weight"].wait()
     kn_scr[...] = unit(
         jnp.dot(normed[...], wk[...], preferred_element_type=F32), key_gain[...]
     ).astype(BF16)
-    loads[2].wait()
+    loads["value_weight"].wait()
     vn_scr[...] = jnp.dot(normed[...], wv[...], preferred_element_type=F32).astype(BF16)
-    loads[3].wait()
+    loads["query_gain"].wait()
+    loads["query_weight"].wait()
     for h in range(heads):
         raw = jnp.dot(
             normed[...], wq[:, h * head : (h + 1) * head], preferred_element_type=F32
@@ -176,8 +202,8 @@
     o_recv[pl.ds(peers, 8)] = jnp.zeros((8, props, head), BF16)
     lse_recv[pl.ds(peers, 8)] = jnp.full((8, 1, 128), NEG_LARGE, F32)
 
-    loads[4].wait()
-    loads[5].wait()
+    for name in ("keys", "logcum", "lengths", "values"):
+        loads[name].wait()
     pl.semaphore_wait(barrier, peers)
 
     def send_out(k):
@@ -278,6 +304,8 @@
     def _(step):
         send_lse((me + step) % peers).start()
 
+    for name in ("accepted", "pending_keys", "pending_values"):
+        loads[name].wait()
     width = heads * props
     q_own = q_scr[my_seq]
     own_rows = pl.ds(pl.multiple_of(my_seq * props, props), props)
@@ -377,6 +405,7 @@
 
     all_but_one(att, 2).wait_recv()
 
+    loads["out_weight"].wait()
     part_t = jnp.zeros((out_weight.shape[0], rows), F32)
     for h in range(heads):
         part_t += dot_last(
@@ -434,44 +463,40 @@
     rows = seqs * props
     peers = seqs * heads
     half = output_weight.shape[1] // 2
-    whole = pl.BlockSpec(memory_space=pltpu.VMEM)
-    scalars = pl.BlockSpec(memory_space=pltpu.SMEM)
-    stay = pl.BlockSpec(memory_space=pl.ANY)
-    operands = [
-        (tokens.reshape(rows, width), stay),
-        (norm_gain.reshape(1, width), whole),
-        (query_weight, stay),
-        (key_weight, stay),
-        (value_weight, stay),
-        (forget_weight.T, whole),
-        (forget_bias, scalars),
-        (query_gain.reshape(1, head), whole),
-        (key_gain.reshape(1, head), whole),
-        (output_weight.T, whole),
-        (cache_keys.reshape(seqs, block, head), stay),
-        (cache_values.reshape(seqs, block, head), stay),
-        (jnp.swapaxes(cache_logcum, 1, 2), whole),
-        (pending_keys.reshape(seqs, taken, head), whole),
-        (pending_values.reshape(seqs, taken, head), whole),
-        (jnp.transpose(pending_logcum, (1, 2, 0)), whole),
-        (lengths, scalars),
-        (accepted, scalars),
-        (accepted.reshape(1, seqs), whole),
-        (parents, whole),
-    ]
+    operands = {
+        "tokens": tokens.reshape(rows, width),
+        "norm_gain": norm_gain.reshape(1, width),
+        "query_weight": query_weight,
+        "key_weight": key_weight,
+        "value_weight": value_weight,
+        "forget": forget_weight.T,
+        "forget_bias": forget_bias,
+        "query_gain": query_gain.reshape(1, head),
+        "key_gain": key_gain.reshape(1, head),
+        "out_weight": output_weight.T,
+        "keys": cache_keys.reshape(seqs, block, head),
+        "values": cache_values.reshape(seqs, block, head),
+        "logcum": jnp.swapaxes(cache_logcum, 1, 2),
+        "pending_keys": pending_keys.reshape(seqs, taken, head),
+        "pending_values": pending_values.reshape(seqs, taken, head),
+        "pending_logcum": jnp.transpose(pending_logcum, (1, 2, 0)),
+        "lengths": lengths,
+        "accepted": accepted,
+        "accepted_row": accepted.reshape(1, seqs),
+        "parents": parents,
+    }
+    places = {
+        name: (pltpu.SMEM if name in SCALARS else pltpu.VMEM)(array.shape, array.dtype)
+        for name, array in operands.items()
+    }
     return pl.pallas_call(
         functools.partial(kernel, seqs, heads, props, head, taken, block),
         out_shape=jax.ShapeDtypeStruct((seqs, props, half), BF16),
-        in_specs=[spec for _, spec in operands],
-        out_specs=whole,
+        in_specs=[{name: pl.BlockSpec(memory_space=pltpu.HBM) for name in operands}],
+        out_specs=pl.BlockSpec(memory_space=pltpu.VMEM),
         scratch_shapes=[
+            places,
             pltpu.VMEM((rows, width), BF16),
-            pltpu.VMEM((rows, width), BF16),
-            pltpu.VMEM((width, heads * head), BF16),
-            pltpu.VMEM((width, head), BF16),
-            pltpu.VMEM((width, head), BF16),
-            pltpu.VMEM((seqs, block, head), BF16),
-            pltpu.VMEM((seqs, block, head), BF16),
             pltpu.VMEM((seqs, heads * props, head), BF16),
             pltpu.VMEM((rows, head), BF16),
             pltpu.VMEM((rows, head), BF16),
@@ -485,14 +510,14 @@
             pltpu.VMEM((peers, props, head), BF16),
             pltpu.VMEM((half, rows), BF16),
             pltpu.VMEM((half, rows), BF16),
-            pltpu.SemaphoreType.DMA((6,)),
+            pltpu.SemaphoreType.DMA((len(operands),)),
             pltpu.SemaphoreType.DMA((4,)),
             pltpu.SemaphoreType.DMA((4,)),
         ],
         compiler_params=pltpu.CompilerParams(
-            collective_id=0, has_side_effects=True, vmem_limit_bytes=48 * 1024 * 1024
+            collective_id=0, has_side_effects=True, vmem_limit_bytes=67043328
         ),
-    )(*[array for array, _ in operands])
+    )(operands)
 
 
 def solution(mesh):

time: 59.7 us -> 45 us (0.75)
  local copies, waits for them, and re-layouts: 15.5 us -> 1.47 us
    unnamed x37 -> x1, local copies, waits for them, and re-layouts: 15.5 us -> 1.47 us
where the time goes in v2:
time: 45 us; the launch traced here: 44.8 us
  Pallas kernels  43.3 us (96%)
  local copies, waits for them, and re-layouts  1.47 us (3%)
    pallas_call x1, Pallas kernels, shards(): pl.pallas_call(functools.partial(kernel, seqs, heads, props, head, taken,...  43.3 us
    unnamed x1, local copies, waits for them, and re-layouts  1.47 us

profile of v2, /device:TPU:1, one launch (start us, length us, event | category | flops | bytes accessed | tf_op | source)
XLA Modules:
  0.0 44.8 jit_solution(1420968413691852599)
XLA Ops:
  0.0 43.3 %shard_map.181 = bf16[16,16,16]{2,1,0:T(8,128)(2,1)} custom-call(s32[16]{0:T(128)} %operands__accepted__.1, s32[1,16]{1,0:T(1,128)} %bitcast.23, bf16[8,2048]{1,0:T(8,128)(2,1)} %bitcast.17, f32[8]{0:T(128)} %operands__forget_bias__.1, f32[1,128]{1,0:T(1,128)} %bitcast.24, bf16[2048,128]{1,0:T(8,128)(2,1)} %operands__key_weight__.1, ...), custom_call_target="tpu_custom_call" | custom-call | tf_op jit(solution)/shard_map/pallas_call | solution.py:492
  43.3 1.5 %copy.21 = bf16[16,16,16]{2,1,0:T(8,128)(2,1)} copy(bf16[16,16,16]{2,1,0:T(8,128)(2,1)} %shard_map.181) | data formatting | bytes 16384

commit v3 on v2

--- a/solution.py
+++ b/solution.py
@@ -10,6 +10,7 @@
 EPSILON = 1e-06
 NEG_LARGE = -1e30
 NEG_FLOOR = -1e29
+ROUNDS = 2
 HIGHEST = lax.Precision.HIGHEST
 MESH = pl.DeviceIdType.MESH
 F32 = jnp.float32
@@ -70,6 +71,10 @@
     return lax.dot_general(a, b, LAST, preferred_element_type=F32)
 
 
+def by_distance(count):
+    return sorted(range(count), key=lambda d: -min(d, count - d))
+
+
 def unit(rows, gain):
     return rows * lax.rsqrt(jnp.mean(rows * rows, axis=-1, keepdims=True) + EPSILON) * gain
 
@@ -85,6 +90,7 @@
     result,
     places,
     normed,
+    scale_scr,
     q_scr,
     kn_scr,
     vn_scr,
@@ -107,9 +113,23 @@
     scaling = head**-0.5
     me = lax.axis_index("kv")
     core = lax.axis_index("tp")
+    across_y = 2 * heads
+    planes = seqs // 2
+    my_z = me // across_y
+    my_y = me & (across_y - 1)
     my_seq = me // heads
-    my_head = me % heads
-
+    my_head = me & (heads - 1)
+    z_at = [((my_z + dz) & (planes - 1)) * across_y for dz in range(planes)]
+    y_at = [(my_y + dy) & (across_y - 1) for dy in range(across_y)]
+    others = sorted(
+        ((dz, dy) for dz in range(planes) for dy in range(across_y) if dz or dy),
+        key=lambda d: -min(d[0], planes - d[0]) - min(d[1], across_y - d[1]),
+    )
+
+    wkv = places["key_weight"]
+    places = dict(
+        places, key_weight=wkv.at[:, pl.ds(0, head)], value_weight=wkv.at[:, pl.ds(head, head)]
+    )
     loads = {
         name: pltpu.make_async_copy(operands[name], places[name], load_sem.at[n])
         for n, name in enumerate(LOAD_ORDER)
@@ -117,19 +137,17 @@
     for item in loads.values():
         item.start()
     (
-        tok, norm_gain, wq, wk, wv, forget, forget_bias, query_gain, key_gain, out_weight,
+        tok, norm_gain, wq, _, _, forget, forget_bias, query_gain, key_gain, out_weight,
         kbuf, vbuf, logcum, pending_keys, pending_values, pending_logcum, lengths, accepted,
         accepted_row, parents,
     ) = (places[name] for name in NAMES)
 
     barrier = pltpu.get_barrier_semaphore()
 
-    @pl.loop(1, peers)
-    def _(step):
+    for dz, dy in others:
         pl.semaphore_signal(
-            barrier, inc=1, device_id={"kv": (me + step) % peers}, device_id_type=MESH
-        )
-
+            barrier, inc=1, device_id={"kv": z_at[dz] + y_at[dy]}, device_id_type=MESH
+        )
     pl.semaphore_signal(barrier, inc=1, device_id={"tp": 1 - core}, device_id_type=MESH)
 
     loads["parents"].wait()
@@ -154,13 +172,33 @@
     loads["tokens"].wait()
     loads["norm_gain"].wait()
 
-    @pl.loop(0, rows // 16)
+    model = tok.shape[1]
+
+    @pl.loop(0, rows // 32)
     def _(step):
-        piece = pl.ds(step * 16, 16)
-        wide = tok[piece, :].astype(F32)
-        normed[piece, :] = unit(wide, norm_gain[...]).astype(BF16)
-
-    for name in ("forget", "forget_bias", "accepted_row", "pending_logcum"):
+        piece = pl.ds(step * 32, 32)
+        total = jnp.zeros((32, 128), F32)
+        for c in range(model // 128):
+            wide = tok[piece, c * 128 : (c + 1) * 128].astype(F32)
+            total += wide * wide
+        scale_scr[piece, :] = total
+
+    mean = jnp.sum(scale_scr[...], axis=1, keepdims=True) * (1.0 / model)
+    scale_scr[...] = jnp.broadcast_to(lax.rsqrt(mean + EPSILON), (rows, 128))
+
+    @pl.loop(0, rows // 32)
+    def _(step):
+        piece = pl.ds(step * 32, 32)
+        scale = scale_scr[piece, :]
+        for c in range(model // 128):
+            columns = slice(c * 128, (c + 1) * 128)
+            wide = tok[piece, columns].astype(F32)
+            normed[piece, columns] = (wide * scale * norm_gain[:, columns]).astype(BF16)
+
+    for name in (
+        "forget", "forget_bias", "accepted_row", "pending_logcum", "key_gain", "query_gain",
+        "key_weight", "value_weight", "query_weight",
+    ):
         loads[name].wait()
     gate_raw = dot_last(forget[...], normed[...])
     gate_head = iota((2 * heads, 1), 0)
@@ -182,30 +220,26 @@
     ) + jnp.dot(base, expand, precision=HIGHEST, preferred_element_type=F32)
     cum_scr[...] = cum_t.T
 
-    loads["key_gain"].wait()
-    loads["key_weight"].wait()
-    kn_scr[...] = unit(
-        jnp.dot(normed[...], wk[...], preferred_element_type=F32), key_gain[...]
-    ).astype(BF16)
-    loads["value_weight"].wait()
-    vn_scr[...] = jnp.dot(normed[...], wv[...], preferred_element_type=F32).astype(BF16)
-    loads["query_gain"].wait()
-    loads["query_weight"].wait()
-    for h in range(heads):
+    sides = jnp.dot(normed[...], wkv[...], preferred_element_type=F32)
+    kn_scr[...] = unit(sides[:, :head], key_gain[...]).astype(BF16)
+    vn_scr[...] = sides[:, head:].astype(BF16)
+    for pair in range(heads // 2):
         raw = jnp.dot(
-            normed[...], wq[:, h * head : (h + 1) * head], preferred_element_type=F32
-        )
-        q_scr[:, h * props : (h + 1) * props, :] = (
-            unit(raw, query_gain[...]).astype(BF16).reshape(seqs, props, head)
-        )
+            normed[...],
+            wq[:, 2 * pair * head : (2 * pair + 2) * head],
+            preferred_element_type=F32,
+        )
+        for h in (2 * pair, 2 * pair + 1):
+            one = raw[:, (h - 2 * pair) * head : (h - 2 * pair + 1) * head]
+            q_scr[:, h * props : (h + 1) * props, :] = (
+                unit(one, query_gain[...]).astype(BF16).reshape(seqs, props, head)
+            )
 
     o_recv[pl.ds(peers, 8)] = jnp.zeros((8, props, head), BF16)
     lse_recv[pl.ds(peers, 8)] = jnp.full((8, 1, 128), NEG_LARGE, F32)
 
     for name in ("keys", "logcum", "lengths", "values"):
         loads[name].wait()
-    pl.semaphore_wait(barrier, peers)
-
     def send_out(k):
         return pltpu.make_async_remote_copy(
             src_ref=o_send.at[k],
@@ -218,7 +252,7 @@
 
     def send_lse(k):
         return pltpu.make_async_remote_copy(
-            src_ref=lse_send.at[k // heads],
+            src_ref=lse_send.at[lax.shift_right_logical(k, heads.bit_length() - 1)],
             dst_ref=lse_recv.at[me],
             send_sem=send_sem.at[1],
             recv_sem=recv_sem.at[1],
@@ -248,17 +282,14 @@
             device_id_type=MESH,
         )
 
-    planes = seqs // 2
-    my_plane = my_seq // 2
     place = me * block + iota((1, block), 1)
-
-    @pl.loop(0, planes // 2, init_carry=jnp.zeros((heads * props, 128), F32))
-    def lse_cols(g, cols):
-        members = []
-        for far in (planes // 2 + g, planes // 2 - 1 - g):
-            plane = (my_plane + far) % planes
-            members += [2 * plane, 2 * plane + 1]
-        for s in members:
+    slot = iota((heads * props, 128), 1)
+    far_first = by_distance(planes)
+    for g in range(ROUNDS):
+        fars = far_first[g * planes // ROUNDS : (g + 1) * planes // ROUNDS]
+        members = [lax.shift_right_logical(z_at[far], heads.bit_length() - 1) + half for far in fars for half in range(2)]
+        cols = jnp.zeros((heads * props, 128), F32)
+        for j, s in enumerate(members):
             raw = dot_last(q_scr[s], kbuf[s])
             minus = jnp.where(place < lengths[s], -logcum[s], NEG_LARGE)
             cum = cum_scr[pl.ds(pl.multiple_of(s * props, props), props), :]
@@ -279,30 +310,22 @@
             out = (out * (1.0 / safe)).astype(BF16)
             o_send[pl.ds(s * heads, heads)] = out.reshape(heads, props, head)
             lse = jnp.where(some, top + jnp.log(safe), NEG_LARGE)
-            cols = jnp.where(iota((heads * props, 128), 1) == s, lse, cols)
-        for s in members:
-            for h in range(heads):
-                k = s * heads + h
-
-                @pl.when(k != me)
-                def _():
-                    send_out(k).start()
-
-                @pl.when(k == me)
-                def _():
-                    o_recv[me] = o_send[k]
-
-        return cols
-
-    padded = jnp.concatenate([lse_cols, jnp.zeros((128 - heads * props, 128), F32)], axis=0)
-    lse_rows = padded.T
-    for s in range(seqs):
-        lse_send[s] = lse_rows[s : s + 1]
+            cols = jnp.where(slot == j, lse, cols)
+        lse_rows = jnp.concatenate(
+            [cols, jnp.zeros((128 - heads * props, 128), F32)], axis=0
+        ).T
+        for j, s in enumerate(members):
+            lse_send[s] = lse_rows[j : j + 1]
+        if g == 0:
+            pl.semaphore_wait(barrier, peers)
+        for far in fars:
+            for dy in by_distance(across_y):
+                if far or dy:
+                    send_out(z_at[far] + y_at[dy]).start()
+                    send_lse(z_at[far] + y_at[dy]).start()
+
+    o_recv[me] = o_send[me]
     lse_recv[me] = lse_send[my_seq]
-
-    @pl.loop(1, peers)
-    def _(step):
-        send_lse((me + step) % peers).start()
 
     for name in ("accepted", "pending_keys", "pending_values"):
         loads[name].wait()
@@ -399,9 +422,8 @@
     )
     att[my_head * seqs + my_seq] = (blended / den).astype(BF16)
 
-    @pl.loop(1, peers)
-    def _(step):
-        send_att((me + step) % peers).start()
+    for dz, dy in others:
+        send_att(z_at[dz] + y_at[dy]).start()
 
     all_but_one(att, 2).wait_recv()
 
@@ -488,7 +510,9 @@
     places = {
         name: (pltpu.SMEM if name in SCALARS else pltpu.VMEM)(array.shape, array.dtype)
         for name, array in operands.items()
+        if name != "value_weight"
     }
+    places["key_weight"] = pltpu.VMEM((width, 2 * head), BF16)
     return pl.pallas_call(
         functools.partial(kernel, seqs, heads, props, head, taken, block),
         out_shape=jax.ShapeDtypeStruct((seqs, props, half), BF16),
@@ -497,6 +521,7 @@
         scratch_shapes=[
             places,
             pltpu.VMEM((rows, width), BF16),
+            pltpu.VMEM((rows, 128), F32),
             pltpu.VMEM((seqs, heads * props, head), BF16),
             pltpu.VMEM((rows, head), BF16),
             pltpu.VMEM((rows, head), BF16),

time: 45 us -> 40 us (0.89)
  Pallas kernels: 43.3 us -> 38.3 us
    pallas_call x1, Pallas kernels: 43.3 us -> 38.3 us  [shards(): pl.pallas_call(functools.partial(kernel, seqs, heads, props, head, taken,...]
where the time goes in v3:
time: 40 us; the launch traced here: 39.8 us
  Pallas kernels  38.3 us (96%)
  local copies, waits for them, and re-layouts  1.47 us (4%)
    pallas_call x1, Pallas kernels, shards(): pl.pallas_call(functools.partial(kernel, seqs, heads, props, head, taken,...  38.3 us
    unnamed x1, local copies, waits for them, and re-layouts  1.47 us

profile of v3, /device:TPU:1, one launch (start us, length us, event | category | flops | bytes accessed | tf_op | source)
XLA Modules:
  0.0 39.8 jit_solution(2181686938535776483)
XLA Ops:
  0.0 38.3 %shard_map.181 = bf16[16,16,16]{2,1,0:T(8,128)(2,1)} custom-call(s32[16]{0:T(128)} %operands__accepted__.1, s32[1,16]{1,0:T(1,128)} %bitcast.23, bf16[8,2048]{1,0:T(8,128)(2,1)} %bitcast.17, f32[8]{0:T(128)} %operands__forget_bias__.1, f32[1,128]{1,0:T(1,128)} %bitcast.24, bf16[2048,128]{1,0:T(8,128)(2,1)} %operands__key_weight__.1, ...), custom_call_target="tpu_custom_call" | custom-call | tf_op jit(solution)/shard_map/pallas_call | solution.py:516
  38.3 1.5 %copy.21 = bf16[16,16,16]{2,1,0:T(8,128)(2,1)} copy(bf16[16,16,16]{2,1,0:T(8,128)(2,1)} %shard_map.181) | data formatting | bytes 16384

commit v4 on v3

--- a/solution.py
+++ b/solution.py
@@ -10,7 +10,7 @@
 EPSILON = 1e-06
 NEG_LARGE = -1e30
 NEG_FLOOR = -1e29
-ROUNDS = 2
+ROUNDS = (2, 2, 4)
 HIGHEST = lax.Precision.HIGHEST
 MESH = pl.DeviceIdType.MESH
 F32 = jnp.float32
@@ -282,11 +282,19 @@
             device_id_type=MESH,
         )
 
+    def send_planes(fars):
+        for far in fars:
+            for dy in by_distance(across_y):
+                if far or dy:
+                    send_out(z_at[far] + y_at[dy]).start()
+                    send_lse(z_at[far] + y_at[dy]).start()
+
     place = me * block + iota((1, block), 1)
     slot = iota((heads * props, 128), 1)
+    late = my_z >= planes // 2
     far_first = by_distance(planes)
-    for g in range(ROUNDS):
-        fars = far_first[g * planes // ROUNDS : (g + 1) * planes // ROUNDS]
+    for g in range(len(ROUNDS)):
+        fars = far_first[sum(ROUNDS[:g]) * planes // 8 : sum(ROUNDS[: g + 1]) * planes // 8]
         members = [lax.shift_right_logical(z_at[far], heads.bit_length() - 1) + half for far in fars for half in range(2)]
         cols = jnp.zeros((heads * props, 128), F32)
         for j, s in enumerate(members):
@@ -316,13 +324,17 @@
         ).T
         for j, s in enumerate(members):
             lse_send[s] = lse_rows[j : j + 1]
-        if g == 0:
-            pl.semaphore_wait(barrier, peers)
-        for far in fars:
-            for dy in by_distance(across_y):
-                if far or dy:
-                    send_out(z_at[far] + y_at[dy]).start()
-                    send_lse(z_at[far] + y_at[dy]).start()
+
+        @pl.when(late)
+        def _():
+            if g == 0:
+                pl.semaphore_wait(barrier, peers)
+            send_planes(fars)
+
+    @pl.when(jnp.logical_not(late))
+    def _():
+        pl.semaphore_wait(barrier, peers)
+        send_planes(far_first)
 
     o_recv[me] = o_send[me]
     lse_recv[me] = lse_send[my_seq]
@@ -540,9 +552,14 @@
             pltpu.SemaphoreType.DMA((4,)),
         ],
         compiler_params=pltpu.CompilerParams(
-            collective_id=0, has_side_effects=True, vmem_limit_bytes=67043328
+            collective_id=0, has_side_effects=True, vmem_limit_bytes=48 * 1024 * 1024
         ),
-    )(operands)
+    )(
+        {
+            name: pltpu.with_memory_space_constraint(array, pltpu.HBM)
+            for name, array in operands.items()
+        }
+    )
 
 
 def solution(mesh):

time: 40 us -> 38.2 us (0.955)
  Pallas kernels: 38.3 us -> 37.4 us
  local copies, waits for them, and re-layouts: 1.47 us -> 0.63 us
    pallas_call x1, Pallas kernels: 38.3 us -> 37.4 us  [shards(): pl.pallas_call(functools.partial(kernel, seqs, heads, props, head, taken,...]
    unnamed x1, local copies, waits for them, and re-layouts: 1.47 us -> 0.63 us
where the time goes in v4:
time: 38.2 us; the launch traced here: 38.1 us
  Pallas kernels  37.4 us (98%)
  local copies, waits for them, and re-layouts  0.63 us (2%)
    pallas_call x1, Pallas kernels, shards(): pl.pallas_call(functools.partial(kernel, seqs, heads, props, head, taken,...  37.4 us

profile of v4, /device:TPU:1, one launch (start us, length us, event | category | flops | bytes accessed | tf_op | source)
XLA Modules:
  0.0 38.1 jit_solution(1668982833954308326)
XLA Ops:
  0.0 37.4 %shard_map.181 = bf16[16,16,16]{2,1,0:T(8,128)(2,1)S(1)} custom-call(s32[16]{0:T(128)} %operands__accepted__.1, s32[1,16]{1,0:T(1,128)} %bitcast.23, bf16[8,2048]{1,0:T(8,128)(2,1)} %bitcast.17, f32[8]{0:T(128)} %operands__forget_bias__.1, f32[1,128]{1,0:T(1,128)} %bitcast.24, bf16[2048,128]{1,0:T(8,128)(2,1)} %operands__key_weight__.1, ...), custom_call_target="tpu_custom_call" | custom-call | tf_op jit(solution)/shard_map/pallas_call | solution.py:528
  37.5 0.6 %copy.21 = bf16[16,16,16]{2,1,0:T(8,128)(2,1)} copy(bf16[16,16,16]{2,1,0:T(8,128)(2,1)S(1)} %shard_map.181) | data formatting | bytes 16384

commit v5 on v4

--- a/solution.py
+++ b/solution.py
@@ -10,7 +10,7 @@
 EPSILON = 1e-06
 NEG_LARGE = -1e30
 NEG_FLOOR = -1e29
-ROUNDS = (2, 2, 4)
+ROUNDS = (2, 2, 2, 2)
 HIGHEST = lax.Precision.HIGHEST
 MESH = pl.DeviceIdType.MESH
 F32 = jnp.float32
@@ -293,12 +293,24 @@
     slot = iota((heads * props, 128), 1)
     late = my_z >= planes // 2
     far_first = by_distance(planes)
-    for g in range(len(ROUNDS)):
-        fars = far_first[sum(ROUNDS[:g]) * planes // 8 : sum(ROUNDS[: g + 1]) * planes // 8]
-        members = [lax.shift_right_logical(z_at[far], heads.bit_length() - 1) + half for far in fars for half in range(2)]
+    far_rounds = [
+        far_first[sum(ROUNDS[:g]) * planes // 8 : sum(ROUNDS[: g + 1]) * planes // 8]
+        for g in range(len(ROUNDS))
+    ]
+    members = [
+        [
+            lax.shift_right_logical(z_at[far], heads.bit_length() - 1) + half
+            for far in fars
+            for half in range(2)
+        ]
+        for fars in far_rounds
+    ]
+    ahead = [dot_last(q_scr[s], kbuf[s]) for s in members[0]]
+    for g, fars in enumerate(far_rounds):
+        raws = ahead
+        ahead = [dot_last(q_scr[s], kbuf[s]) for s in members[g + 1]] if g + 1 < len(members) else []
         cols = jnp.zeros((heads * props, 128), F32)
-        for j, s in enumerate(members):
-            raw = dot_last(q_scr[s], kbuf[s])
+        for j, (s, raw) in enumerate(zip(members[g], raws)):
             minus = jnp.where(place < lengths[s], -logcum[s], NEG_LARGE)
             cum = cum_scr[pl.ds(pl.multiple_of(s * props, props), props), :]
             scores = jnp.concatenate(
@@ -312,17 +324,18 @@
             top = jnp.maximum(jnp.max(scores, axis=-1, keepdims=True), NEG_FLOOR)
             weights = jnp.exp(scores - top)
             total = jnp.sum(weights, axis=-1, keepdims=True)
-            some = total > 0.0
-            safe = jnp.where(some, total, 1.0)
             out = jnp.dot(weights.astype(BF16), vbuf[s], preferred_element_type=F32)
-            out = (out * (1.0 / safe)).astype(BF16)
+            out = (out * (1.0 / jnp.maximum(total, 1.0))).astype(BF16)
             o_send[pl.ds(s * heads, heads)] = out.reshape(heads, props, head)
-            lse = jnp.where(some, top + jnp.log(safe), NEG_LARGE)
-            cols = jnp.where(slot == j, lse, cols)
-        lse_rows = jnp.concatenate(
+            cols = jnp.where(slot == j, top, jnp.where(slot == 16 + j, total, cols))
+        turned = jnp.concatenate(
             [cols, jnp.zeros((128 - heads * props, 128), F32)], axis=0
         ).T
-        for j, s in enumerate(members):
+        totals = turned[16:32]
+        lse_rows = jnp.where(
+            totals > 0.0, turned[:16] + jnp.log(jnp.maximum(totals, 1.0)), NEG_LARGE
+        )
+        for j, s in enumerate(members[g]):
             lse_send[s] = lse_rows[j : j + 1]
 
         @pl.when(late)

time: 38.2 us -> 37.4 us (0.979)
  Pallas kernels: 37.4 us -> 36.6 us
    pallas_call x1, Pallas kernels: 37.4 us -> 36.6 us  [shards(): pl.pallas_call(functools.partial(kernel, seqs, heads, props, head, taken,...]
where the time goes in v5:
time: 37.4 us; the launch traced here: 37.3 us
  Pallas kernels  36.6 us (98%)
  local copies, waits for them, and re-layouts  0.63 us (2%)
    pallas_call x1, Pallas kernels, shards(): pl.pallas_call(functools.partial(kernel, seqs, heads, props, head, taken,...  36.6 us

profile of v5, /device:TPU:1, one launch (start us, length us, event | category | flops | bytes accessed | tf_op | source)
XLA Modules:
  0.0 37.3 jit_solution(2784805757446598298)
XLA Ops:
  0.0 36.6 %shard_map.181 = bf16[16,16,16]{2,1,0:T(8,128)(2,1)S(1)} custom-call(s32[16]{0:T(128)} %operands__accepted__.1, s32[1,16]{1,0:T(1,128)} %bitcast.23, bf16[8,2048]{1,0:T(8,128)(2,1)} %bitcast.17, f32[8]{0:T(128)} %operands__forget_bias__.1, f32[1,128]{1,0:T(1,128)} %bitcast.24, bf16[2048,128]{1,0:T(8,128)(2,1)} %operands__key_weight__.1, ...), custom_call_target="tpu_custom_call" | custom-call | tf_op jit(solution)/shard_map/pallas_call | solution.py:541
  36.6 0.6 %copy.21 = bf16[16,16,16]{2,1,0:T(8,128)(2,1)} copy(bf16[16,16,16]{2,1,0:T(8,128)(2,1)S(1)} %shard_map.181) | data formatting | bytes 16384

commit v6 on v5

--- a/solution.py
+++ b/solution.py
@@ -160,14 +160,22 @@
     parent_row = jnp.sum(
         jnp.where(lane // props == iota((seqs, rows), 0), repeated, 0.0), axis=0, keepdims=True
     ).astype(jnp.int32)
-    down = iota((rows, rows), 0)
-    across = iota((rows, rows), 1)
+    side = anc_scr.shape[1]
+    down = iota((side, side), 0)
+    across = iota((side, side), 1)
     same = down // props == across // props
-    linked = (same & (parent_row == (down & (props - 1)))) | (down == across)
-    anc_t = jnp.where(linked, 1.0, 0.0).astype(BF16)
-    for _ in range((props - 1).bit_length()):
-        anc_t = jnp.minimum(jnp.dot(anc_t, anc_t, preferred_element_type=F32), 1.0).astype(BF16)
-    anc_scr[...] = anc_t
+    anc_t = []
+    for start in range(0, rows, side):
+        linked = (same & (parent_row[:, start : start + side] == (down & (props - 1)))) | (
+            down == across
+        )
+        reach = jnp.where(linked, 1.0, 0.0).astype(BF16)
+        for _ in range((props - 1).bit_length()):
+            reach = jnp.minimum(
+                jnp.dot(reach, reach, preferred_element_type=F32), 1.0
+            ).astype(BF16)
+        anc_scr[start : start + side, :] = reach
+        anc_t.append(reach)
 
     loads["tokens"].wait()
     loads["norm_gain"].wait()
@@ -215,8 +223,17 @@
         base = jnp.where(accepted_row[...] - 1 == a, pending_logcum[a], base)
     base = jnp.concatenate([base, jnp.zeros((heads, seqs), F32)], axis=0)
     expand = (lane // props == iota((seqs, rows), 0)).astype(F32)
-    cum_t = jnp.dot(
-        gates, anc_t.astype(F32), precision=HIGHEST, preferred_element_type=F32
+    cum_t = jnp.concatenate(
+        [
+            jnp.dot(
+                gates[:, n * side : (n + 1) * side],
+                reach.astype(F32),
+                precision=HIGHEST,
+                preferred_element_type=F32,
+            )
+            for n, reach in enumerate(anc_t)
+        ],
+        axis=1,
     ) + jnp.dot(base, expand, precision=HIGHEST, preferred_element_type=F32)
     cum_scr[...] = cum_t.T
 
@@ -286,8 +303,8 @@
         for far in fars:
             for dy in by_distance(across_y):
                 if far or dy:
+                    send_lse(z_at[far] + y_at[dy]).start()
                     send_out(z_at[far] + y_at[dy]).start()
-                    send_lse(z_at[far] + y_at[dy]).start()
 
     place = me * block + iota((1, block), 1)
     slot = iota((heads * props, 128), 1)
@@ -386,7 +403,7 @@
         jnp.where(lane_prop == iota((props, width), 0), cum_wide, 0.0), axis=0, keepdims=True
     )
     anc_fold = (
-        (iota((rows, width), 0) & (props - 1)) == (iota((rows, width), 1) & (props - 1))
+        (iota((side, width), 0) & (props - 1)) == (iota((side, width), 1) & (props - 1))
     ).astype(BF16)
     anc_own = jnp.dot(anc_scr[own_rows, :], anc_fold, preferred_element_type=F32)
     pend_wide = jnp.zeros((extra, width), F32)
@@ -550,7 +567,7 @@
             pltpu.VMEM((seqs, heads * props, head), BF16),
             pltpu.VMEM((rows, head), BF16),
             pltpu.VMEM((rows, head), BF16),
-            pltpu.VMEM((rows, rows), BF16),
+            pltpu.VMEM((rows, min(rows, 128)), BF16),
             pltpu.VMEM((rows, 2 * heads), F32),
             pltpu.VMEM((peers, props, head), BF16),
             pltpu.VMEM((peers + 8, props, head), BF16),

time: 37.4 us -> 37.2 us (level)
  no operation moved by 1% of the time
where the time goes in v6:
time: 37.2 us; the launch traced here: 37 us
  Pallas kernels  36.4 us (98%)
  local copies, waits for them, and re-layouts  0.63 us (2%)
    pallas_call x1, Pallas kernels, shards(): pl.pallas_call(functools.partial(kernel, seqs, heads, props, head, taken,...  36.4 us

profile of v6, /device:TPU:1, one launch (start us, length us, event | category | flops | bytes accessed | tf_op | source)
XLA Modules:
  0.0 37.0 jit_solution(1382547578967062949)
XLA Ops:
  0.0 36.4 %shard_map.181 = bf16[16,16,16]{2,1,0:T(8,128)(2,1)S(1)} custom-call(s32[16]{0:T(128)} %operands__accepted__.1, s32[1,16]{1,0:T(1,128)} %bitcast.23, bf16[8,2048]{1,0:T(8,128)(2,1)} %bitcast.17, f32[8]{0:T(128)} %operands__forget_bias__.1, f32[1,128]{1,0:T(1,128)} %bitcast.24, bf16[2048,128]{1,0:T(8,128)(2,1)} %operands__key_weight__.1, ...), custom_call_target="tpu_custom_call" | custom-call | tf_op jit(solution)/shard_map/pallas_call | solution.py:558
  36.4 0.6 %copy.21 = bf16[16,16,16]{2,1,0:T(8,128)(2,1)} copy(bf16[16,16,16]{2,1,0:T(8,128)(2,1)S(1)} %shard_map.181) | data formatting | bytes 16384

commit v7 on v6

--- a/solution.py
+++ b/solution.py
@@ -439,16 +439,16 @@
     lse_t = top_t + jnp.log(total_t)
     lse_recv[peers] = jnp.concatenate([lse_t, jnp.zeros((1, 128 - width), F32)], axis=1)
 
-    all_but_one(lse_recv, 1).wait_recv()
     slots = peers + 8
-    lse_all = lse_recv[:, 0, :]
-    weight = jnp.exp(lse_all - jnp.max(lse_all, axis=0, keepdims=True)).astype(BF16)
     pick = (
         (iota((128, 128), 0) - my_head * props) == (iota((128, 128), 1) & (props - 1))
     ).astype(BF16)
-    picked = jnp.dot(weight, pick, preferred_element_type=F32)
     mine_8 = iota((8, 128), 1) // props == iota((8, 128), 0)
     mine_16 = (iota((props, 128), 1) & (props - 1)) == iota((props, 128), 0)
+    all_but_one(lse_recv, 1).wait_recv()
+    lse_all = lse_recv[:, 0, :]
+    weight = jnp.exp(lse_all - jnp.max(lse_all, axis=0, keepdims=True)).astype(BF16)
+    picked = jnp.dot(weight, pick, preferred_element_type=F32)
     mixes = []
     for c in range(slots // 8):
         flat = jnp.sum(

time: 37.2 us -> 37.2 us (level)
  no operation moved by 1% of the time
where the time goes in v7:
time: 37.2 us; the launch traced here: 37 us
  Pallas kernels  36.4 us (98%)
  local copies, waits for them, and re-layouts  0.63 us (2%)
    pallas_call x1, Pallas kernels, shards(): pl.pallas_call(functools.partial(kernel, seqs, heads, props, head, taken,...  36.4 us

profile of v7, /device:TPU:1, one launch (start us, length us, event | category | flops | bytes accessed | tf_op | source)
XLA Modules:
  0.0 37.0 jit_solution(14143546326068721250)
XLA Ops:
  0.0 36.4 %shard_map.181 = bf16[16,16,16]{2,1,0:T(8,128)(2,1)S(1)} custom-call(s32[16]{0:T(128)} %operands__accepted__.1, s32[1,16]{1,0:T(1,128)} %bitcast.23, bf16[8,2048]{1,0:T(8,128)(2,1)} %bitcast.17, f32[8]{0:T(128)} %operands__forget_bias__.1, f32[1,128]{1,0:T(1,128)} %bitcast.24, bf16[2048,128]{1,0:T(8,128)(2,1)} %operands__key_weight__.1, ...), custom_call_target="tpu_custom_call" | custom-call | tf_op jit(solution)/shard_map/pallas_call | solution.py:558
  36.4 0.6 %copy.21 = bf16[16,16,16]{2,1,0:T(8,128)(2,1)} copy(bf16[16,16,16]{2,1,0:T(8,128)(2,1)S(1)} %shard_map.181) | data formatting | bytes 16384
